TPU v7x, 32 devices: a whole 2x2x4 slice. The times are simulated.
32 devices in a mesh: sp: 8 (over z, core), tp: 4 (over y, x).
Axes of the slice: x: 2, y: 2, z: 4, core: 2. Of those that a mesh axis runs over, the one named last changes fastest.
Arguments:
- query_a: bfloat16 [1536, 2048], P('sp', 'tp'), may hold values from -6 to 6
- key_a: bfloat16 [1536, 2048], P('sp', 'tp'), may hold values from -6 to 6
- value_a: bfloat16 [1536, 2048], P('sp', 'tp'), may hold values from -6 to 6
- query_b: bfloat16 [1536, 2048], P('sp', 'tp'), may hold values from -6 to 6
- key_b: bfloat16 [1536, 2048], P('sp', 'tp'), may hold values from -6 to 6
- value_b: bfloat16 [1536, 2048], P('sp', 'tp'), may hold values from -6 to 6
- stop_a: float32 [1536, 32], P('sp', 'tp'), may hold values from -14 to -1
- stop_b: float32 [1536, 16], P('sp', 'tp'), may hold values from -14 to -1
- out_a: bfloat16 [2048, 2048], P('tp'), may hold values from -4 to 4
- out_b: bfloat16 [2048, 2048], P('tp'), may hold values from -4 to 4
- resid: bfloat16 [1536, 2048], P('sp', 'tp'), may hold values from -20 to 20
- mix_gain: float32 [2048], P('tp'), may hold values from 0.1 to 1.9
- ffn_gain: float32 [2048], P('tp'), may hold values from 0.1 to 1.9
- routes: int32 [1536, 2], P('sp'), may hold values from 0 to 31, all different within a row; in each aligned block of 192 rows (0 to 191, 192 to 383, ...) at most 18 rows name the same one
- gates: float32 [1536, 2], P('sp'), may hold values from 0.25 to 1.5
- exp_gate: bfloat16 [32, 2048, 512], P('sp', 'tp'), may hold values from -0.125 to 0.125
- exp_up: bfloat16 [32, 2048, 512], P('sp', 'tp'), may hold values from -0.125 to 0.125
- exp_down: bfloat16 [32, 512, 2048], P('sp', None, 'tp'), may hold values from -0.25 to 0.25
- sh_gate: bfloat16 [2048, 512], P('tp'), may hold values from -0.125 to 0.125
- sh_up: bfloat16 [2048, 512], P('tp'), may hold values from -0.125 to 0.125
- sh_down: bfloat16 [512, 2048], P(None, 'tp'), may hold values from -4 to 4
Outputs:
- result: bfloat16 [1536, 2048], P('sp', 'tp')
Inputs may be any that keep to these rules, and one draw needn't show every extreme that they name: `routes`: each row names 2 different experts. Within the rows of one index of sp (aligned blocks of 192 rows) no expert is named by more than 18 rows, a bound that some block reaches.
All inputs are finite; a program needn't handle non-finite values.
Results may differ from a plain program's by a relative error of at most 0.02.
Values may be sent and summed in bfloat16 or wider, within the bound.
A program may use at most 64 MiB of HBM per device.

v0:
```python
import functools

import jax
import jax.numpy as jnp
import numpy as np
from jax import lax
from jax.experimental import pallas as pl
from jax.experimental.pallas import tpu as pltpu
from jax.sharding import PartitionSpec as P

MESH = pl.DeviceIdType.MESH
LANES = 128
LOG2E = 1.4426950408889634
epsilon = 1e-06
VM = pl.BlockSpec(memory_space=pltpu.VMEM)


def greet(axis, peers):
    barrier = pltpu.get_barrier_semaphore()
    for peer in peers:
        pl.semaphore_signal(barrier, inc=1, device_id={axis: peer}, device_id_type=MESH)
    pl.semaphore_wait(barrier, len(peers))


def params(cid):
    return pltpu.CompilerParams(
        collective_id=cid, has_side_effects=True, vmem_limit_bytes=56 * 1024 * 1024
    )


def snake(r, j, m):
    return m * r + (j if m % 2 == 0 else r - 1 - j)


def stick_kernel(n, rows, groups, offsets, *refs):
    g_count = len(groups)
    count = 3 * g_count + 1
    ins, outs = refs[:count], refs[count : count + g_count]
    full = refs[count + g_count : 2 * count + g_count]
    made = refs[2 * count + g_count : 2 * count + 2 * g_count]
    send, recv, rsend, rrecv, own, bsend, brecv = refs[2 * count + 2 * g_count :]
    me = lax.axis_index("sp")
    nz = n // 2
    z, c = me // 2, lax.rem(me, 2)
    partner = z * 2 + 1 - c
    places = [lax.rem(z + d, nz) for d in range(nz)]
    greet("sp", [lax.rem(me + d, n) for d in range(1, n)])
    order = [count - 1] + list(range(count - 1))

    def piece(t, place):
        if t == count - 1:
            return ins[t]
        unit = (2 * place) // (n // groups[t // 3][0])
        return ins[t].at[:, pl.ds(pl.multiple_of(unit * LANES, LANES), LANES)]

    def spot(t, source):
        tall = ins[t].shape[0]
        return full[t].at[pl.ds(pl.multiple_of(source * tall, tall), tall), :]

    def remote(source, target, send_sem, recv_sem, device):
        copy = pltpu.make_async_remote_copy(
            src_ref=source,
            dst_ref=target,
            send_sem=send_sem,
            recv_sem=recv_sem,
            device_id={"sp": device},
            device_id_type=MESH,
        )
        copy.start()
        return copy

    first, relays, local = {}, {}, {}
    for t in order:
        for d in range(1, nz):
            first[d, t] = remote(
                piece(t, places[d]), spot(t, me), send.at[d, t], recv.at[d, t], places[d] * 2 + c
            )
        relays[0, t] = remote(piece(t, z), spot(t, me), rsend.at[0, t], rrecv.at[0, t], partner)
        local[t] = pltpu.make_async_copy(piece(t, z), spot(t, me), own.at[t])
        local[t].start()

    def relay(d, t):
        source = lax.rem(z + nz - d, nz) * 2 + c
        first[d, t].wait_recv()
        relays[d, t] = remote(
            spot(t, source), spot(t, source), rsend.at[d, t], rrecv.at[d, t], partner
        )

    def arrive(t):
        local[t].wait()
        for d in range(nz):
            relays[d, t].wait_recv()

    group_arrays = lambda g: ([count - 1] if g == 0 else []) + [3 * g, 3 * g + 1, 3 * g + 2]
    for d in range(1, nz):
        for t in group_arrays(0):
            relay(d, t)

    tile = 2 * LANES
    upper = (
        lax.broadcasted_iota(jnp.int32, (tile, tile), 0)
        > lax.broadcasted_iota(jnp.int32, (tile, tile), 1)
    ).astype(jnp.bfloat16)
    lane = lax.broadcasted_iota(jnp.int32, (rows, LANES), 1)
    column = lax.broadcasted_iota(jnp.int32, (rows, tile), 1)
    line = lax.broadcasted_iota(jnp.int32, (rows, tile), 0)
    backs = []
    for g in range(g_count):
        units, size = groups[g]
        q_ref, k_ref, v_ref = full[3 * g : 3 * g + 3]
        r = n // units
        unit, j = me // r, lax.rem(me, r)
        heads = LANES // size
        scale = LOG2E * size ** (-0.5)
        for t in group_arrays(g):
            arrive(t)
        pending = []
        if g + 1 < g_count:
            pending = [(d, t) for d in range(1, nz) for t in group_arrays(g + 1)]
        for m in range(n // r):
            block = snake(r, j, m)
            last = lambda b: ((b + 1) * rows - 1) // tile
            counts = [last(snake(r, jj, m)) + 1 for jj in range(r)]
            query = q_ref[pl.ds(pl.multiple_of(block * rows, rows), rows), :]
            lines = ins[count - 1].shape[0]
            stop_t = full[count - 1][pl.ds(pl.multiple_of(block * lines, lines), lines), :]
            fill = jnp.zeros((LANES - lines, stop_t.shape[1]), jnp.float32)
            stop_all = jnp.concatenate([stop_t, fill], axis=0).T[:rows]
            parts = []
            for h in range(heads):
                head = offsets[g] + unit * heads + h
                stop = jnp.sum(jnp.where(lane == head, stop_all, 0.0), axis=1, keepdims=True) * LOG2E
                if heads > 1:
                    mine = query * ((lane // size) == h).astype(jnp.bfloat16)
                else:
                    mine = query
                carry = jnp.zeros((rows, 1), jnp.float32)
                total = jnp.zeros((rows, LANES), jnp.float32)
                for i in range(max(counts)):
                    where_tile = (block * rows + rows - 1) // tile - i
                    masked = i < 2 or i >= min(counts)
                    start = pl.multiple_of(jnp.maximum(where_tile, 0) * tile, tile)
                    keys = k_ref[pl.ds(start, tile), :]
                    values = v_ref[pl.ds(start, tile), :]
                    score = lax.dot_general(
                        mine, keys, (((1,), (1,)), ((), ())), preferred_element_type=jnp.float32
                    )
                    score = score * scale + stop
                    small = jnp.log2(1.0 + jnp.exp2(-jnp.abs(score)))
                    fail = jnp.maximum(score, 0.0) + small
                    hit = score - fail
                    if masked:
                        valid = column + where_tile * tile < line + block * rows
                        if i >= min(counts):
                            valid = jnp.logical_and(valid, where_tile >= 0)
                        fail = jnp.where(valid, fail, 0.0)
                    high = fail.astype(jnp.bfloat16)
                    low = (fail - high.astype(jnp.float32)).astype(jnp.bfloat16)
                    after = jnp.dot(high, upper, preferred_element_type=jnp.float32) + jnp.dot(
                        low, upper, preferred_element_type=jnp.float32
                    )
                    weight = jnp.exp2(hit - after - carry)
                    if masked:
                        weight = jnp.where(valid, weight, 0.0)
                    carry = carry + after[:, :1] + fail[:, :1]
                    total = total + jnp.dot(
                        weight.astype(jnp.bfloat16), values, preferred_element_type=jnp.float32
                    )
                parts.append(total)
            merged = parts[0]
            for h in range(1, heads):
                merged = jnp.where(lane // size >= h, parts[h], merged)
            made[g][m] = merged.astype(jnp.bfloat16)
            place = outs[g].at[:, pl.ds(pl.multiple_of(unit * LANES, LANES), LANES)]

            @pl.when(block != me)
            def _():
                pltpu.make_async_remote_copy(
                    src_ref=made[g].at[m],
                    dst_ref=place,
                    send_sem=bsend.at[g, m],
                    recv_sem=brecv.at[g, unit],
                    device_id={"sp": block},
                    device_id_type=MESH,
                ).start()

            @pl.when(block == me)
            def _():
                pltpu.make_async_copy(made[g].at[m], place, bsend.at[g, m]).start()

            share = -(-len(pending) // (n // r - m))
            for d, t in pending[:share]:
                relay(d, t)
            pending = pending[share:]

    for g in range(g_count):
        r = n // groups[g][0]
        turn, rest = me // r, lax.rem(me, r)
        owner = jnp.where(lax.rem(turn, 2) == 0, rest, r - 1 - rest)
        for u in range(groups[g][0]):

            @pl.when(u * r + owner != me)
            def _(g=g, u=u):
                place = outs[g].at[:, pl.ds(u * LANES, LANES)]
                pltpu.make_async_copy(place, place, brecv.at[g, u]).wait()

        unit = me // r
        place = outs[g].at[:, pl.ds(pl.multiple_of(unit * LANES, LANES), LANES)]
        for m in range(groups[g][0]):
            pltpu.make_async_copy(made[g].at[m], place, bsend.at[g, m]).wait()
    for copy in first.values():
        copy.wait_send()
    for copy in relays.values():
        copy.wait_send()


def stick(n, rows, arrays, groups, offsets, cid):
    k, g_count = len(arrays), len(groups)
    nz, top = n // 2, max(units for units, _ in groups)
    dma = pltpu.SemaphoreType.DMA
    return pl.pallas_call(
        functools.partial(stick_kernel, n, rows, groups, offsets),
        out_shape=tuple(
            jax.ShapeDtypeStruct((rows, units * LANES), jnp.bfloat16) for units, _ in groups
        ),
        in_specs=[VM] * k,
        out_specs=[VM] * g_count,
        scratch_shapes=[
            pltpu.VMEM((n * a.shape[0], LANES if i < k - 1 else a.shape[1]), a.dtype)
            for i, a in enumerate(arrays)
        ]
        + [pltpu.VMEM((units, rows, LANES), jnp.bfloat16) for units, _ in groups]
        + [dma((nz, k))] * 4
        + [dma((k,)), dma((g_count, top)), dma((g_count, top))],
        compiler_params=params(cid),
        name="stick",
    )(*arrays)


def exchange_kernel(axis, n, modes, *refs):
    count = len(modes)
    ins, outs = refs[:count], refs[count : 2 * count]
    send, recv = refs[2 * count :]
    me = lax.axis_index(axis)
    greet(axis, [lax.rem(me + d, n) for d in range(1, n)])

    def ends(t, peer):
        if modes[t] == "lead":
            return ins[t].at[peer], outs[t].at[me]
        if modes[t] == "cols":
            width = ins[t].shape[1] // n
            return ins[t].at[:, pl.ds(pl.multiple_of(peer * width, width), width)], outs[t].at[me]
        if modes[t] == "all":
            return ins[t], outs[t].at[me]
        width = ins[t].shape[1]
        return ins[t], outs[t].at[:, pl.ds(pl.multiple_of(me * width, width), width)]

    copies = []
    for d in range(1, n):
        peer = lax.rem(me + d, n)
        for t in range(count):
            source, target = ends(t, peer)
            copies.append(
                pltpu.make_async_remote_copy(
                    src_ref=source,
                    dst_ref=target,
                    send_sem=send.at[d, t],
                    recv_sem=recv.at[d, t],
                    device_id={axis: peer},
                    device_id_type=MESH,
                )
            )
            copies[-1].start()
    for t in range(count):
        source, target = ends(t, me)
        copies.append(pltpu.make_async_copy(source, target, send.at[0, t]))
        copies[-1].start()
    for copy in copies:
        copy.wait()


def exchange(axis, n, arrays, modes, cid):
    def shape(a, mode):
        if mode == "lead":
            return a.shape
        if mode == "cols":
            return (n, a.shape[0], a.shape[1] // n)
        if mode == "all":
            return (n,) + a.shape
        return (a.shape[0], a.shape[1] * n)

    if modes[0] == "cols" and any((a.shape[1] // n) % LANES for a in arrays):
        cut = [jnp.transpose(a.reshape(a.shape[0], n, -1), (1, 0, 2)) for a in arrays]
        return exchange(axis, n, cut, ("lead",) * len(cut), cid)
    if modes[0] == "side" and any(a.shape[1] % LANES for a in arrays):
        stacked = exchange(axis, n, arrays, ("all",) * len(arrays), cid)
        return [jnp.transpose(a, (1, 0, 2)).reshape(a.shape[1], -1) for a in stacked]
    k = len(arrays)
    return pl.pallas_call(
        functools.partial(exchange_kernel, axis, n, modes),
        out_shape=tuple(jax.ShapeDtypeStruct(shape(a, m), a.dtype) for a, m in zip(arrays, modes)),
        in_specs=[VM] * k,
        out_specs=[VM] * k,
        scratch_shapes=[pltpu.SemaphoreType.DMA((n, k))] * 2,
        compiler_params=params(cid),
        name="exchange",
    )(*arrays)


def moe_kernel(
    n_sp,
    n_tp,
    out_ref,
    normed_ref,
    stream_ref,
    slot_ref,
    gates_ref,
    gather_ref,
    scatter_ref,
    gate_ref,
    up_ref,
    down_ref,
    sg_ref,
    su_ref,
    sd_ref,
    result_ref,
    arrived,
    returned,
    made,
    pre,
    pre_in,
    hid,
    s_pre,
    s_pre_in,
    s_hid,
    weights,
    load_sem,
    dsend,
    drecv,
    bsend,
    brecv,
    psend,
    precv,
    hsend,
    hrecv,
):
    f32, bf16 = jnp.float32, jnp.bfloat16
    me, col = lax.axis_index("sp"), lax.axis_index("tp")
    nz = n_sp // 2
    z = me // 2
    experts = gate_ref.shape[0]
    width = hid.shape[2] // n_tp
    block = arrived.shape[1]
    loads = [
        pltpu.make_async_copy(ref, weights.at[i], load_sem.at[i])
        for i, ref in enumerate((gate_ref, up_ref, down_ref))
    ]
    for load in loads:
        load.start()
    barrier = pltpu.get_barrier_semaphore()
    for d in range(1, n_sp):
        pl.semaphore_signal(
            barrier, inc=1, device_id={"sp": lax.rem(me + d, n_sp)}, device_id_type=MESH
        )
    for d in range(1, n_tp):
        pl.semaphore_signal(
            barrier, inc=1, device_id={"tp": lax.rem(col + d, n_tp)}, device_id_type=MESH
        )
    pl.semaphore_wait(barrier, n_sp + n_tp - 2)

    def dot(a, b):
        return jnp.dot(a, b, preferred_element_type=f32)

    def slab(which):
        return pl.ds(pl.multiple_of(which * width, width), width)

    sends = []

    def remote(source, target, send, recv, where):
        copy = pltpu.make_async_remote_copy(
            src_ref=source,
            dst_ref=target,
            send_sem=send,
            recv_sem=recv,
            device_id=where,
            device_id_type=MESH,
        )
        copy.start()
        sends.append(copy)

    for d in range(1, n_sp):
        peer = lax.rem(me + d, n_sp)
        remote(out_ref.at[peer], arrived.at[me], dsend.at[d], drecv.at[me], {"sp": peer})
    own_in = pltpu.make_async_copy(out_ref.at[me], arrived.at[me], drecv.at[me])
    own_in.start()

    offsets = [0] + [o for d in range(1, nz // 2 + 1) for o in dict.fromkeys((d, nz - d))]
    chips = [lax.rem(z + o, nz) for o in offsets]
    shared = len(chips)

    def buffers(c):
        if c == shared:
            return s_pre, s_pre_in, s_hid
        return pre.at[c], pre_in.at[c], hid.at[c]

    def send_pre(c):
        here, there, _ = buffers(c)
        for d in range(1, n_tp):
            peer = lax.rem(col + d, n_tp)
            for k in range(2):
                remote(
                    here.at[k, :, slab(peer)],
                    there.at[d - 1, k],
                    psend.at[c, d - 1, k],
                    precv.at[c, d - 1, k],
                    {"tp": peer},
                )

    def first(c):
        here, _, _ = buffers(c)
        if c == shared:
            rows = normed_ref[...]
            here[0] = dot(rows, sg_ref[...]).astype(bf16)
            here[1] = dot(rows, su_ref[...]).astype(bf16)
        else:
            grouped = None
            for k in range(2):
                source = chips[c] * 2 + k
                slot = arrived.at[source]
                pltpu.make_async_copy(slot, slot, drecv.at[source]).wait()
                term = dot(gather_ref[:, k * LANES : k * LANES + block], arrived[source])
                grouped = term if grouped is None else grouped + term
            grouped = grouped.astype(bf16)
            tall = grouped.shape[0] // experts
            if c == 0:
                loads[0].wait()
                loads[1].wait()
            for k in range(2):
                parts = [
                    dot(grouped[e * tall : (e + 1) * tall], weights[k, e]).astype(bf16)
                    for e in range(experts)
                ]
                spread_rows = jnp.concatenate(parts, axis=0)
                here[k] = jnp.concatenate(
                    [dot(scatter_ref[j], spread_rows) for j in range(2)], axis=0
                ).astype(bf16)
        send_pre(c)

    def second(c):
        here, there, full = buffers(c)
        sums = []
        for k in range(2):
            total = here[k, :, slab(col)].astype(f32)
            for d in range(1, n_tp):
                slot = there.at[d - 1, k]
                pltpu.make_async_copy(slot, slot, precv.at[c, d - 1, k]).wait()
                total = total + there[d - 1, k].astype(f32)
            sums.append(total)
        full[:, slab(col)] = (sums[0] / (1.0 + jnp.exp(-sums[0])) * sums[1]).astype(bf16)
        for d in range(1, n_tp):
            peer = lax.rem(col + d, n_tp)
            mine = full.at[:, slab(col)]
            remote(mine, mine, hsend.at[c, d - 1], hrecv.at[c, d - 1], {"tp": peer})

    def third(c):
        _, _, full = buffers(c)
        for d in range(1, n_tp):
            slot = full.at[:, slab(lax.rem(col + n_tp - d, n_tp))]
            pltpu.make_async_copy(slot, slot, hrecv.at[c, d - 1]).wait()
        if c == shared:
            result_sum = dot(full[...], sd_ref[...])
            return result_sum
        hidden = full[...]
        grouped = dot(gather_ref[:, :block], hidden[:block]) + dot(
            gather_ref[:, LANES : LANES + block], hidden[block:]
        )
        grouped = grouped.astype(bf16)
        tall = grouped.shape[0] // experts
        if c == 0:
            loads[2].wait()
        parts = [
            dot(grouped[e * tall : (e + 1) * tall], weights[2, e]).astype(bf16)
            for e in range(experts)
        ]
        parts = jnp.concatenate(parts, axis=0)
        for k in range(2):
            source = chips[c] * 2 + k
            made[c, k] = dot(scatter_ref[k], parts).astype(bf16)
            if c == 0:

                @pl.when(source != me)
                def _():
                    pltpu.make_async_remote_copy(
                        src_ref=made.at[c, k],
                        dst_ref=returned.at[me],
                        send_sem=bsend.at[c, k],
                        recv_sem=brecv.at[me],
                        device_id={"sp": source},
                        device_id_type=MESH,
                    ).start()

                @pl.when(source == me)
                def _():
                    pltpu.make_async_copy(made.at[c, k], returned.at[me], brecv.at[me]).start()

            else:
                remote(
                    made.at[c, k], returned.at[me], bsend.at[c, k], brecv.at[me], {"sp": source}
                )
        return None

    first(shared)
    first(0)
    second(shared)
    for c in range(shared + 2):
        if 1 <= c < shared:
            first(c)
        if 1 <= c <= shared:
            second(c - 1)
        if c == 1:
            total = third(shared) + stream_ref[...].astype(f32)
        if c >= 2:
            third(c - 2)
    for chip in chips:
        for k in range(2):
            source = chip * 2 + k
            slot = returned.at[source]
            pltpu.make_async_copy(slot, slot, brecv.at[source]).wait()
            rows = returned[source]
            seats = source * block + lax.broadcasted_iota(jnp.int32, (total.shape[0], block), 1)
            gated = jnp.zeros(seats.shape, f32)
            for t in range(slot_ref.shape[1]):
                gated = gated + jnp.where(
                    seats == slot_ref[:, t : t + 1], gates_ref[:, t : t + 1], 0.0
                )
            high = gated.astype(bf16)
            low = (gated - high.astype(f32)).astype(bf16)
            total = total + dot(high, rows) + dot(low, rows)
    result_ref[...] = total.astype(bf16)
    for copy in sends:
        copy.wait_send()
    for k in range(2):

        @pl.when(chips[0] * 2 + k != me)
        def _():
            pltpu.make_async_copy(made.at[0, k], made.at[0, k], bsend.at[0, k]).wait()


def moe_fused(n_sp, n_tp, outgoing, normed, stream, slot, gates, capacity, mats, shared_mats, cid):
    bf16 = jnp.bfloat16
    experts, hidden_width = mats[0].shape[0], mats[0].shape[2]
    block, width = outgoing.shape[1], outgoing.shape[2]
    rows = normed.shape[0]
    nz = n_sp // 2
    tall = -(-2 * capacity // 16) * 16
    index = np.arange(block)
    gather = np.zeros((experts * tall, 2 * LANES), np.float32)
    scatter = np.zeros((2, block, experts * tall), np.float32)
    for k in range(2):
        place = index // capacity * tall + k * capacity + index % capacity
        gather[place, k * LANES + index] = 1.0
        scatter[k, index, place] = 1.0
    part = hidden_width // n_tp
    dma = pltpu.SemaphoreType.DMA
    anywhere = pl.BlockSpec(memory_space=pl.ANY)
    return pl.pallas_call(
        functools.partial(moe_kernel, n_sp, n_tp),
        out_shape=jax.ShapeDtypeStruct((rows, width), bf16),
        in_specs=[VM] * 7 + [anywhere] * 3 + [VM] * 3,
        out_specs=VM,
        scratch_shapes=[
            pltpu.VMEM((n_sp, block, width), bf16),
            pltpu.VMEM((n_sp, block, width), bf16),
            pltpu.VMEM((nz, 2, block, width), bf16),
            pltpu.VMEM((nz, 2, 2 * block, hidden_width), bf16),
            pltpu.VMEM((nz, n_tp - 1, 2, 2 * block, part), bf16),
            pltpu.VMEM((nz, 2 * block, hidden_width), bf16),
            pltpu.VMEM((2, rows, hidden_width), bf16),
            pltpu.VMEM((n_tp - 1, 2, rows, part), bf16),
            pltpu.VMEM((rows, hidden_width), bf16),
            pltpu.VMEM((3,) + mats[0].shape, bf16),
            dma((3,)),
            dma((n_sp,)),
            dma((n_sp,)),
            dma((nz, 2)),
            dma((n_sp,)),
            dma((nz + 1, n_tp - 1, 2)),
            dma((nz + 1, n_tp - 1, 2)),
            dma((nz + 1, n_tp - 1)),
            dma((nz + 1, n_tp - 1)),
        ],
        compiler_params=params(cid),
        name="moe",
    )(
        outgoing,
        normed,
        stream,
        slot,
        gates,
        jnp.asarray(gather, bf16),
        jnp.asarray(scatter, bf16),
        *mats,
        *shared_mats,
    )


def shards(
    n_sp,
    n_tp,
    query_a,
    key_a,
    value_a,
    query_b,
    key_b,
    value_b,
    stop_a,
    stop_b,
    out_a,
    out_b,
    resid,
    mix_gain,
    ffn_gain,
    routes,
    gates,
    exp_gate,
    exp_up,
    exp_down,
    sh_gate,
    sh_up,
    sh_down,
):
    f32, bf16 = jnp.float32, jnp.bfloat16
    rows = query_a.shape[0]
    heads_a, heads_b = stop_a.shape[1], stop_b.shape[1]
    units_a, units_b = query_a.shape[1] // LANES, query_b.shape[1] // LANES
    width = resid.shape[1]
    model = width * n_tp

    local_experts = exp_gate.shape[0]
    experts = local_experts * n_sp
    top_count = routes.shape[1]
    capacity = max(1, (3 * rows * top_count + 2 * experts - 1) // (2 * experts))
    flat_routes = routes.reshape(-1)
    onehot = (flat_routes[:, None] == jnp.arange(experts, dtype=jnp.int32)[None, :]).astype(f32)
    pairs = rows * top_count
    before = (jnp.arange(pairs)[:, None] > jnp.arange(pairs)[None, :]).astype(bf16)
    earlier = jnp.dot(before, onehot.astype(bf16), preferred_element_type=f32)
    slot = flat_routes * capacity + jnp.sum(earlier * onehot, axis=1).astype(jnp.int32)
    slot = slot.reshape(rows, top_count)
    slots = jnp.arange(experts * capacity, dtype=jnp.int32)
    block = local_experts * capacity
    hidden_width = exp_gate.shape[2]
    fused = (
        (hidden_width // n_tp) % LANES == 0
        and block % 8 == 0
        and block <= LANES
        and exp_gate.shape == exp_down.shape
    )
    chosen = slot[:, :, None] == slots[None, None, :]
    chooser = jnp.sum(chosen.astype(f32), axis=1).astype(bf16)
    gated = jnp.sum(jnp.where(chosen, gates[:, :, None], 0.0), axis=1)
    gated_high = gated.astype(bf16)
    gated_low = (gated - gated_high.astype(f32)).astype(bf16)

    stops = jnp.concatenate([stop_a, stop_b], axis=1)
    lines = -(-stops.shape[1] // 8) * 8
    wide = -(-rows // LANES) * LANES
    stops = jnp.pad(stops.T, ((0, lines - stops.shape[1]), (0, wide - rows)))
    groups = ((units_a, query_a.shape[1] // heads_a), (units_b, query_b.shape[1] // heads_b))
    arrays = (query_a, key_a, value_a, query_b, key_b, value_b, stops)
    attended_a, attended_b = stick(n_sp, rows, arrays, groups, (0, heads_a), 0)

    partial_value = jnp.dot(attended_a, out_a, preferred_element_type=f32)
    partial_value = partial_value + jnp.dot(attended_b, out_b, preferred_element_type=f32)
    (pieces,) = exchange("tp", n_tp, (partial_value.astype(bf16),), ("cols",), 2)
    mixed = jnp.sum(pieces.astype(f32), axis=0)
    resid_f = resid.astype(f32)
    shaped = mixed * mix_gain[None, :]
    sums = jnp.stack(
        [
            jnp.sum(mixed * mixed, axis=1),
            jnp.sum(resid_f * resid_f, axis=1),
            jnp.sum(resid_f * shaped, axis=1),
            jnp.sum(shaped * shaped, axis=1),
        ]
    )
    sums = jnp.pad(sums, ((0, 4), (0, wide - rows)))
    (sums,) = exchange("tp", n_tp, (sums,), ("all",), 3)
    sums = jnp.sum(sums, axis=0)[:4, :rows]
    scale = lax.rsqrt(sums[0] / model + epsilon)
    stream = (resid_f + shaped * scale[:, None]).astype(bf16)
    square = jnp.maximum(sums[1] + scale * (2.0 * sums[2] + scale * sums[3]), 0.0)
    stream_f = stream.astype(f32)
    normed = (stream_f * lax.rsqrt(square / model + epsilon)[:, None] * ffn_gain[None, :]).astype(bf16)

    outgoing = lax.dot_general(chooser, normed, (((0,), (0,)), ((), ())), preferred_element_type=f32)
    outgoing = outgoing.astype(bf16).reshape(n_sp, local_experts * capacity, width)
    if fused:
        return moe_fused(
            n_sp,
            n_tp,
            outgoing,
            normed,
            stream,
            slot,
            gates,
            capacity,
            (exp_gate, exp_up, exp_down),
            (sh_gate, sh_up, sh_down),
            8,
        )
    (arrived,) = exchange("sp", n_sp, (outgoing,), ("lead",), 4)
    arrived = arrived.reshape(n_sp, local_experts, capacity, width)
    arrived = jnp.transpose(arrived, (1, 0, 2, 3)).reshape(local_experts, n_sp * capacity, width)

    shared_parts = [
        jnp.dot(normed, w, preferred_element_type=f32).astype(bf16) for w in (sh_gate, sh_up)
    ]
    expert_parts = [
        jnp.einsum("erd,edf->erf", arrived, w, preferred_element_type=f32)
        .astype(bf16)
        .reshape(local_experts * n_sp * capacity, -1)
        for w in (exp_gate, exp_up)
    ]
    parts = exchange("tp", n_tp, (*expert_parts, *shared_parts), ("cols",) * 4, 5)
    gate_pre, up_pre, shared_gate, shared_up = [jnp.sum(p.astype(f32), axis=0) for p in parts]
    hidden = (jax.nn.silu(gate_pre) * up_pre).astype(bf16)
    shared_hidden = (jax.nn.silu(shared_gate) * shared_up).astype(bf16)
    hidden, shared_hidden = exchange("tp", n_tp, (hidden, shared_hidden), ("side",) * 2, 6)

    shared_out = jnp.dot(shared_hidden, sh_down, preferred_element_type=f32)
    hidden = hidden.reshape(local_experts, n_sp * capacity, -1)
    produced = jnp.einsum("erf,efd->erd", hidden, exp_down, preferred_element_type=f32).astype(bf16)
    produced = produced.reshape(local_experts, n_sp, capacity, width)
    produced = jnp.transpose(produced, (1, 0, 2, 3)).reshape(n_sp, local_experts * capacity, width)
    (returned,) = exchange("sp", n_sp, (produced,), ("lead",), 7)
    flat_back = returned.reshape(experts * capacity, width)
    routed = jnp.dot(gated_high, flat_back, preferred_element_type=f32)
    routed = routed + jnp.dot(gated_low, flat_back, preferred_element_type=f32)
    moe = routed + shared_out
    return (stream_f + moe).astype(bf16)


def solution(mesh):
    return jax.shard_map(
        functools.partial(shards, mesh.shape["sp"], mesh.shape["tp"]),
        mesh=mesh,
        in_specs=(
            P("sp", "tp"),
            P("sp", "tp"),
            P("sp", "tp"),
            P("sp", "tp"),
            P("sp", "tp"),
            P("sp", "tp"),
            P("sp", "tp"),
            P("sp", "tp"),
            P("tp", None),
            P("tp", None),
            P("sp", "tp"),
            P("tp"),
            P("tp"),
            P("sp", None),
            P("sp", None),
            P("sp", "tp", None),
            P("sp", "tp", None),
            P("sp", None, "tp"),
            P("tp", None),
            P("tp", None),
            P(None, "tp"),
        ),
        out_specs=P("sp", "tp"),
        check_vma=False,
    )
```

profile of v0, /device:TPU:1, one launch (start us, length us, event | category | flops | bytes accessed | tf_op | source)
XLA Modules:
  0.0 135.8 jit_solution(11382061112060377682)
XLA Ops:
  0.0 0.0 copy-start
  0.0 0.9 maximum_bitcast_fusion
  0.9 0.6 pad.8.refs_6_
  1.5 51.2 %stick.1 = (bf16[192,512]{1,0:T(8,128)(2,1)}, bf16[192,512]{1,0:T(8,128)(2,1)}) custom-call(bf16[192,512]{1,0:T(8,128)(2,1)} %refs_0_.1, bf16[192,512]{1,0:T(8,128)(2,1)} %refs_1_.1, bf16[192,512]{1,0:T(8,128)(2,1)} %refs_2_.1, bf16[192,512]{1,0:T(8,128)(2,1)} %refs_3_.1, bf16[192,512]{1,0:T(8,128)(2,1)} %refs_4_.1, bf16[192,512]{1,0:T(8,128)(2,1)} %refs_5_.1, ...), custom_call_target="tpu_custom_call" | custom-call | tf_op jit(solution)/shard_map/stick/pallas_call | solution.py:221
  52.7 0.0 copy-start.1
  52.7 0.0 copy-start.5
  52.8 0.0 copy-done
  52.8 1.7 %fusion.11 = f32[192,2048]{1,0:T(8,128)S(1)} fusion(bf16[192,512]{1,0:T(8,128)(2,1)} %get-tuple-element.7, bf16[512,2048]{1,0:T(8,128)(2,1)S(1)} %copy-done), kind=kOutput, calls=%fused_computation.35 | convolution fusion | flops 402653184 | bytes 3866624 | tf_op jit(solution)/shard_map/dot_general | solution.py:673
  54.4 0.0 copy-done.1
  54.4 0.0 copy-done.5
  54.4 1.5 %fusion.refs_0_ = bf16[192,2048]{1,0:T(8,128)(2,1)} fusion(f32[192,2048]{1,0:T(8,128)S(1)} %fusion.11, bf16[192,512]{1,0:T(8,128)(2,1)S(1)} %copy-done.5, bf16[512,2048]{1,0:T(8,128)(2,1)S(1)} %copy-done.1), kind=kOutput, calls=%fused_computation.1 | convolution fusion | flops 403439616 | bytes 4653056 | tf_op jit(solution)/shard_map/dot_general | solution.py:674
  56.0 0.0 copy-start.4
  56.0 0.0 copy-start.6
  56.0 0.0 copy-start.8
  56.0 0.0 copy-start.7
  56.0 14.2 %exchange.2 = bf16[4,192,512]{2,1,0:T(8,128)(2,1)} custom-call(bf16[192,2048]{1,0:T(8,128)(2,1)} %fusion.refs_0_), custom_call_target="tpu_custom_call" | custom-call | tf_op jit(solution)/shard_map/exchange/pallas_call | solution.py:299
  70.1 1.3 convert_reduce_fusion
  71.4 0.0 copy-done.4
  71.4 0.0 copy-done.6
  71.5 0.0 copy-start.9
  71.5 0.2 fusion.3
  71.7 0.6 select_maximum_fusion.refs_0_
  72.3 4.9 %exchange.3 = f32[4,8,256]{2,1,0:T(8,128)} custom-call(f32[8,256]{1,0:T(8,128)} %select_maximum_fusion.refs_0_), custom_call_target="tpu_custom_call" | custom-call | tf_op jit(solution)/shard_map/exchange/pallas_call | solution.py:299
  77.2 0.8 reduce_sum.79
  78.0 0.0 copy-done.8
  78.0 0.8 multiply_convert_fusion
  78.9 0.0 copy-start.2
  78.9 0.0 copy-done.7
  78.9 0.1 copy.36
  79.0 0.1 eq.28
  79.1 0.2 fusion.1
  79.4 0.1 convert_element_type.50
  79.5 0.1 copy.37
  79.7 0.0 copy-start.3
  79.7 0.1 copy.38
  79.7 0.2 convert_reduce_fusion.1
  79.9 1.2 convolution_convert_fusion
  81.1 0.0 copy-done.9
  81.1 0.8 copy.39.gates_ref
  81.8 0.0 copy-done.2
  81.8 0.0 copy-done.3
  81.9 52.3 %moe.1 = bf16[192,512]{1,0:T(8,128)(2,1)} custom-call(bf16[8,72,512]{2,1,0:T(8,128)(2,1)} %bitcast.17, bf16[192,512]{1,0:T(8,128)(2,1)} %copy-done.2, bf16[192,512]{1,0:T(8,128)(2,1)} %get-tuple-element.14.stream_ref, s32[192,2]{1,0:T(8,128)} %copy-done.3, f32[192,2]{1,0:T(8,128)} %copy.39.gates_ref, bf16[192,256]{1,0:T(8,128)(2,1)} %constant.20.clone.gather_ref, ...), custom_call_target="tpu_custom_call" | custom-call | tf_op jit(solution)/shard_map/moe/pallas_call | solution.py:566
  134.2 1.6 %copy.41 = bf16[192,512]{1,0:T(8,128)(2,1)} copy(bf16[192,512]{1,0:T(8,128)(2,1)} %moe.1) | data formatting | bytes 393216
  (5 shorter events, 0.0 us)
Async XLA Ops:
  0.0 52.8 %copy-start = (bf16[512,2048]{1,0:T(8,128)(2,1)S(1)}, bf16[512,2048]{1,0:T(8,128)(2,1)}, u32[]{:S(2)}) copy-start(bf16[512,2048]{1,0:T(8,128)(2,1)} %param.31) | copy-start | bytes 6291460
  52.7 1.7 %copy-start.1 = (bf16[512,2048]{1,0:T(8,128)(2,1)S(1)}, bf16[512,2048]{1,0:T(8,128)(2,1)}, u32[]{:S(2)}) copy-start(bf16[512,2048]{1,0:T(8,128)(2,1)} %param.32) | copy-start | bytes 6291460
  52.7 1.7 %copy-start.5 = (bf16[192,512]{1,0:T(8,128)(2,1)S(1)}, bf16[192,512]{1,0:T(8,128)(2,1)}, u32[]{:S(2)}) copy-start(bf16[192,512]{1,0:T(8,128)(2,1)} %get-tuple-element.8) | copy-start | bytes 589828
  56.0 15.5 %copy-start.4 = (bf16[192,512]{1,0:T(8,128)(2,1)S(1)}, bf16[192,512]{1,0:T(8,128)(2,1)}, u32[]{:S(2)}) copy-start(bf16[192,512]{1,0:T(8,128)(2,1)} %param.33) | copy-start | bytes 589828
  56.0 15.5 %copy-start.6 = (f32[512]{0:T(512)S(1)}, f32[512]{0:T(512)}, u32[]{:S(2)}) copy-start(f32[512]{0:T(512)} %param.34) | copy-start | bytes 6148
  56.0 22.1 %copy-start.8 = (f32[512]{0:T(512)S(1)}, f32[512]{0:T(512)}, u32[]{:S(2)}) copy-start(f32[512]{0:T(512)} %param.35) | copy-start | bytes 6148
  56.0 22.9 %copy-start.7 = (s32[192,2]{0,1:T(2,128)S(1)}, s32[192,2]{0,1:T(2,128)}, u32[]{:S(2)}) copy-start(s32[192,2]{0,1:T(2,128)} %param.36) | copy-start | bytes 4612
  71.5 9.6 %copy-start.9 = (f32[192,2]{0,1:T(2,128)S(1)}, f32[192,2]{0,1:T(2,128)}, u32[]{:S(2)}) copy-start(f32[192,2]{0,1:T(2,128)} %param.37) | copy-start | bytes 4612
  78.9 3.0 %copy-start.2 = (bf16[192,512]{1,0:T(8,128)(2,1)}, bf16[192,512]{1,0:T(8,128)(2,1)S(1)}, u32[]{:S(2)}) copy-start(bf16[192,512]{1,0:T(8,128)(2,1)S(1)} %get-tuple-element.13.normed_ref) | copy-start | bytes 589828
  79.7 2.2 %copy-start.3 = (s32[192,2]{1,0:T(8,128)}, s32[192,2]{1,0:T(8,128)S(1)}, u32[]{:S(2)}) copy-start(s32[192,2]{1,0:T(8,128)S(1)} %add.48.slot_ref) | copy-start | bytes 4612
where the time goes:
time: 136 us
  Pallas kernels  123 us (90%)
  other arithmetic  4.85 us (4%)
  matrix products  4.52 us (3%)
  local copies, waits for them, and re-layouts  3.62 us (3%)
    pallas_call x1, Pallas kernels, moe_fused(): pl.pallas_call(functools.partial(moe_kernel, n_sp, n_tp), out_shape=jax.S...  52.3 us
    pallas_call x1, Pallas kernels, stick(): pl.pallas_call(functools.partial(stick_kernel, n, rows, groups, offsets),...  51.2 us
    pallas_call x2, Pallas kernels, exchange(): pl.pallas_call(functools.partial(exchange_kernel, axis, n, modes), out_sh...  19.1 us

commit v1 on v0

--- a/solution.py
+++ b/solution.py
@@ -1,4 +1,5 @@
 import functools
+import math
 
 import jax
 import jax.numpy as jnp
@@ -307,56 +308,60 @@
     )(*arrays)
 
 
-def moe_kernel(
-    n_sp,
-    n_tp,
-    out_ref,
-    normed_ref,
-    stream_ref,
-    slot_ref,
-    gates_ref,
-    gather_ref,
-    scatter_ref,
-    gate_ref,
-    up_ref,
-    down_ref,
-    sg_ref,
-    su_ref,
-    sd_ref,
-    result_ref,
-    arrived,
-    returned,
-    made,
-    pre,
-    pre_in,
-    hid,
-    s_pre,
-    s_pre_in,
-    s_hid,
-    weights,
-    load_sem,
-    dsend,
-    drecv,
-    bsend,
-    brecv,
-    psend,
-    precv,
-    hsend,
-    hrecv,
-):
+def flip(z, offset):
+    other, bit = z, 1
+    while bit <= offset:
+        if offset & bit:
+            other = other + bit - 2 * bit * lax.rem(z // bit, 2)
+        bit *= 2
+    return other
+
+
+def layer_kernel(n_sp, n_tp, groups, capacity, order, *refs):
     f32, bf16 = jnp.float32, jnp.bfloat16
+    pieces, refs = refs[:6], refs[6:]
+    (stop_a, stop_b, routes_ref, gates_ref, mix_gain, ffn_gain), refs = refs[:6], refs[6:]
+    large, refs = refs[:9], refs[9:]
+    result_ref, refs = refs[0], refs[1:]
+    full, refs = refs[:7], refs[7:]
+    made, refs = refs[:2], refs[2:]
+    attended, refs = refs[:2], refs[2:]
+    held, refs = refs[:9], refs[9:]
+    (stops_own, partial, part_out, part_in, aux, stats_out, stats_in, normed_ref), refs = (
+        refs[:8],
+        refs[8:],
+    )
+    (out_ref, arrived, returned, made_back, pre, pre_in, hid, s_pre, s_pre_in, s_hid), refs = (
+        refs[:10],
+        refs[10:],
+    )
+    (gather_ref, scatter_ref), refs = refs[:2], refs[2:]
+    (load_sem, fsend, frecv, rsend, rrecv, osend, orecv, xsend, xrecv, tsend, trecv), refs = (
+        refs[:11],
+        refs[11:],
+    )
+    dsend, drecv, bsend, brecv, psend, precv, hsend, hrecv = refs
+
     me, col = lax.axis_index("sp"), lax.axis_index("tp")
     nz = n_sp // 2
-    z = me // 2
-    experts = gate_ref.shape[0]
-    width = hid.shape[2] // n_tp
+    z, c = me // 2, lax.rem(me, 2)
+    partner = z * 2 + 1 - c
+    rows = pieces[0].shape[0]
+    tall_rows = rows // LANES * LANES + (LANES if rows % LANES else 0)
+    w_out_a, w_out_b, resid_ref, w_gate, w_up, w_down, sg_ref, su_ref, sd_ref = held
+    experts = w_gate.shape[0]
+    width = resid_ref.shape[1]
     block = arrived.shape[1]
-    loads = [
-        pltpu.make_async_copy(ref, weights.at[i], load_sem.at[i])
-        for i, ref in enumerate((gate_ref, up_ref, down_ref))
-    ]
-    for load in loads:
-        load.start()
+    part = hid.shape[2] // n_tp
+
+    def dot(a, b):
+        return jnp.dot(a, b, preferred_element_type=f32)
+
+    loads = [pltpu.make_async_copy(a, b, load_sem.at[i]) for i, (a, b) in enumerate(zip(large, held))]
+    stops_own[...] = jnp.zeros_like(stops_own)
+    heads_a, heads_b = stop_a.shape[0], stop_b.shape[0]
+    stops_own[:heads_a, :rows] = stop_a[...]
+    stops_own[heads_a : heads_a + heads_b, :rows] = stop_b[...]
     barrier = pltpu.get_barrier_semaphore()
     for d in range(1, n_sp):
         pl.semaphore_signal(
@@ -367,12 +372,6 @@
             barrier, inc=1, device_id={"tp": lax.rem(col + d, n_tp)}, device_id_type=MESH
         )
     pl.semaphore_wait(barrier, n_sp + n_tp - 2)
-
-    def dot(a, b):
-        return jnp.dot(a, b, preferred_element_type=f32)
-
-    def slab(which):
-        return pl.ds(pl.multiple_of(which * width, width), width)
 
     sends = []
 
@@ -388,112 +387,341 @@
         copy.start()
         sends.append(copy)
 
-    for d in range(1, n_sp):
-        peer = lax.rem(me + d, n_sp)
-        remote(out_ref.at[peer], arrived.at[me], dsend.at[d], drecv.at[me], {"sp": peer})
-    own_in = pltpu.make_async_copy(out_ref.at[me], arrived.at[me], drecv.at[me])
-    own_in.start()
-
-    offsets = [0] + [o for d in range(1, nz // 2 + 1) for o in dict.fromkeys((d, nz - d))]
-    chips = [lax.rem(z + o, nz) for o in offsets]
+    def landed(ref, sem):
+        pltpu.make_async_copy(ref, ref, sem).wait()
+
+    ins = tuple(pieces) + (stops_own,)
+    names = ((6, 0, 1, 2), (3, 4, 5))
+
+    def piece(t, place):
+        if t == 6:
+            return ins[t]
+        return ins[t].at[:, pl.ds(pl.multiple_of(place * LANES, LANES), LANES)]
+
+    def spot(t, source):
+        tall = ins[t].shape[0]
+        return full[t].at[pl.ds(pl.multiple_of(source * tall, tall), tall), :]
+
+    places = [flip(z, o) for o in range(nz)]
+    for g in range(2):
+        for t in names[g]:
+            for o in range(1, nz):
+                remote(
+                    piece(t, places[o]),
+                    spot(t, me),
+                    fsend.at[o, t],
+                    frecv.at[z, t],
+                    {"sp": places[o] * 2 + c},
+                )
+            pltpu.make_async_copy(piece(t, z), spot(t, me), frecv.at[z, t]).start()
+    for load in loads:
+        load.start()
+
+    def relay(g, chip):
+        for t in names[g]:
+            mine = spot(t, chip * 2 + c)
+            landed(mine, frecv.at[chip, t])
+            remote(mine, mine, rsend.at[chip, t], rrecv.at[chip, t], {"sp": partner})
+
+    def relayed(g, chip):
+        for t in names[g]:
+            landed(spot(t, chip * 2 + 1 - c), rrecv.at[chip, t])
+
+    slot_rows = []
+
+    def tables():
+        total_experts = n_sp * experts
+        kinds = lax.broadcasted_iota(jnp.int32, (total_experts, rows), 0)
+        hots = [(kinds == routes_ref[t : t + 1, :]).astype(f32) for t in range(routes_ref.shape[0])]
+        named = hots[0]
+        for hot in hots[1:]:
+            named = named + hot
+        before = (
+            lax.broadcasted_iota(jnp.int32, (rows, rows), 0)
+            < lax.broadcasted_iota(jnp.int32, (rows, rows), 1)
+        ).astype(bf16)
+        earlier = dot(named.astype(bf16), before)
+        aux[...] = jnp.zeros_like(aux)
+        for t, hot in enumerate(hots):
+            rank = jnp.sum(earlier * hot, axis=0, keepdims=True)
+            slot = routes_ref[t : t + 1, :].astype(f32) * float(capacity) + rank
+            slot_rows.append(slot)
+            aux[t : t + 1, :rows] = slot
+            aux[len(hots) + t : len(hots) + t + 1, :rows] = gates_ref[t : t + 1, :]
+        spread = gather_ref.shape[0]
+        tall = spread // experts
+
+        def where_of(index, k):
+            place = index + k * capacity
+            for e in range(1, experts):
+                place = place + jnp.where(index >= e * capacity, tall - capacity, 0)
+            return place
+
+        for k in range(2):
+            index = lax.broadcasted_iota(jnp.int32, (spread, LANES), 1)
+            hit = where_of(index, k) == lax.broadcasted_iota(jnp.int32, (spread, LANES), 0)
+            hit = jnp.logical_and(hit, index < block)
+            gather_ref[:, k * LANES : (k + 1) * LANES] = hit.astype(f32).astype(bf16)
+            index = lax.broadcasted_iota(jnp.int32, (block, spread), 0)
+            hit = where_of(index, k) == lax.broadcasted_iota(jnp.int32, (block, spread), 1)
+            scatter_ref[k] = hit.astype(f32).astype(bf16)
+
+    tile = 2 * LANES
+    upper = (
+        lax.broadcasted_iota(jnp.int32, (tile, tile), 0)
+        > lax.broadcasted_iota(jnp.int32, (tile, tile), 1)
+    ).astype(bf16)
+    lane = lax.broadcasted_iota(jnp.int32, (rows, LANES), 1)
+    column = lax.broadcasted_iota(jnp.int32, (rows, tile), 1)
+    line = lax.broadcasted_iota(jnp.int32, (rows, tile), 0)
+
+    backs = []
+    steps = [(g, m) for g in range(2) for m in range(nz)]
+    offsets = (0, heads_a)
+    relay(0, 0)
+    tables()
+    relayed(0, 0)
+    for number, (g, m) in enumerate(steps):
+        size = groups[g][1]
+        heads = LANES // size
+        q_ref, k_ref, v_ref = full[3 * g : 3 * g + 3]
+        scale = LOG2E * size ** (-0.5)
+        block_q = 2 * m + (c if m % 2 == 0 else 1 - c)
+        count = -(-(2 * m + 2) * rows // tile)
+        query = q_ref[pl.ds(pl.multiple_of(block_q * rows, rows), rows), :]
+        lines = stops_own.shape[0]
+        stop_t = full[6][pl.ds(pl.multiple_of(block_q * lines, lines), lines), :]
+        fill = jnp.zeros((LANES - lines, stop_t.shape[1]), f32)
+        stop_all = jnp.concatenate([stop_t, fill], axis=0).T[:rows]
+        parts = []
+        for h in range(heads):
+            head = offsets[g] + z * heads + h
+            stop = jnp.sum(jnp.where(lane == head, stop_all, 0.0), axis=1, keepdims=True) * LOG2E
+            mine = query * ((lane // size) == h).astype(bf16) if heads > 1 else query
+            carry = jnp.zeros((rows, 1), f32)
+            total = jnp.zeros((rows, LANES), f32)
+            for i in range(count):
+                if h == heads - 1 and i == count // 2 and number + 1 < len(steps):
+                    relay(*steps[number + 1])
+                begin = block_q * rows + rows - tile * (i + 1)
+                short = (2 * m + 1) * rows - tile * (i + 1) < 0
+                short = short or (2 * m + 2) * rows - tile * (i + 1) < 0
+                masked = i == 0 or short
+                start = pl.multiple_of(jnp.maximum(begin, 0), math.gcd(rows, tile))
+                keys = k_ref[pl.ds(start, tile), :]
+                values = v_ref[pl.ds(start, tile), :]
+                score = lax.dot_general(
+                    mine, keys, (((1,), (1,)), ((), ())), preferred_element_type=f32
+                )
+                score = score * scale + stop
+                small = jnp.log2(1.0 + jnp.exp2(-jnp.abs(score)))
+                fail = jnp.maximum(score, 0.0) + small
+                hit = score - fail
+                if masked:
+                    valid = column < begin + tile - start
+                    if i == 0:
+                        valid = column + start < line + block_q * rows
+                    fail = jnp.where(valid, fail, 0.0)
+                high = fail.astype(bf16)
+                low = (fail - high.astype(f32)).astype(bf16)
+                after = dot(high, upper) + dot(low, upper)
+                weight = jnp.exp2(hit - after - carry)
+                if masked:
+                    weight = jnp.where(valid, weight, 0.0)
+                carry = carry + after[:, :1] + fail[:, :1]
+                total = total + dot(weight.astype(bf16), values)
+            parts.append(total)
+        merged = parts[0]
+        for h in range(1, heads):
+            merged = jnp.where(lane // size >= h, parts[h], merged)
+        made[g][m] = merged.astype(bf16)
+        place = attended[g].at[:, pl.ds(pl.multiple_of(z * LANES, LANES), LANES)]
+        backs.append((g, m, block_q))
+
+        @pl.when(block_q != me)
+        def _(g=g, m=m, place=place, block_q=block_q):
+            pltpu.make_async_remote_copy(
+                src_ref=made[g].at[m],
+                dst_ref=place,
+                send_sem=osend.at[g, m],
+                recv_sem=orecv.at[g, z],
+                device_id={"sp": block_q},
+                device_id_type=MESH,
+            ).start()
+
+        @pl.when(block_q == me)
+        def _(g=g, m=m, place=place):
+            pltpu.make_async_copy(made[g].at[m], place, orecv.at[g, z]).start()
+
+        if number + 1 < len(steps):
+            relayed(*steps[number + 1])
+
+    loads[0].wait()
+    loads[1].wait()
+    loads[2].wait()
+
+    def columns(which, wide):
+        return pl.ds(pl.multiple_of(which * wide, wide), wide)
+
+    peers = [lax.rem(col + d, n_tp) for d in range(1, n_tp)] + [col]
+    for g, weights in enumerate((w_out_a, w_out_b)):
+        for u in range(groups[g][0]):
+            landed(attended[g].at[:, u * LANES : (u + 1) * LANES], orecv.at[g, u])
+        left = attended[g][...]
+        for i, peer in enumerate(peers):
+            term = dot(left, weights[:, columns(peer, width)])
+            if g == 0:
+                partial[i] = term
+                continue
+            part_out[i] = (partial[i] + term).astype(bf16)
+            if i < n_tp - 1:
+                remote(part_out.at[i], part_in.at[i], xsend.at[i], xrecv.at[i], {"tp": peer})
+    resid = resid_ref[...].astype(f32)
+    mixed = part_out[n_tp - 1].astype(f32)
+    for i in range(n_tp - 1):
+        landed(part_in.at[i], xrecv.at[i])
+        mixed = mixed + part_in[i].astype(f32)
+
+    shaped = mixed * mix_gain[...]
+    sums = jnp.zeros((rows, LANES), f32)
+    for i, term in enumerate((mixed * mixed, resid * resid, resid * shaped, shaped * shaped)):
+        sums = jnp.where(lane == i, jnp.sum(term, axis=1, keepdims=True), sums)
+    if tall_rows > rows:
+        sums = jnp.concatenate([sums, jnp.zeros((tall_rows - rows, LANES), f32)], axis=0)
+    stats_out[...] = sums.T[:8]
+    for d in range(1, n_tp):
+        remote(
+            stats_out, stats_in.at[d - 1], tsend.at[d - 1], trecv.at[d - 1], {"tp": peers[d - 1]}
+        )
+    sums = stats_out[...]
+    for d in range(1, n_tp):
+        landed(stats_in.at[d - 1], trecv.at[d - 1])
+        sums = sums + stats_in[d - 1]
+    sums = jnp.concatenate([sums, jnp.zeros((LANES - 8, tall_rows), f32)], axis=0).T[:rows]
+    model = width * n_tp
+    scale = lax.rsqrt(sums[:, 0:1] / model + epsilon)
+    stream = (resid + shaped * scale).astype(bf16)
+    square = sums[:, 1:2] + scale * (2.0 * sums[:, 2:3] + scale * sums[:, 3:4])
+    square = jnp.maximum(square, 0.0)
+    stream = stream.astype(f32)
+    result_ref[...] = stream
+    normed = stream * lax.rsqrt(square / model + epsilon) * ffn_gain[...]
+    normed_ref[...] = normed.astype(bf16)
+
+    chips = [flip(z, o) for o in order]
     shared = len(chips)
-
-    def buffers(c):
-        if c == shared:
+    seat = lax.broadcasted_iota(jnp.int32, (block, rows), 0)
+    for i, o in enumerate(order):
+        for k in range(2):
+            peer = chips[i] * 2 + lax.rem(c + k, 2)
+            seats = (seat + peer * block).astype(f32)
+            chosen = seats == slot_rows[0]
+            for slot in slot_rows[1:]:
+                chosen = jnp.logical_or(chosen, seats == slot)
+            picked = dot(chosen.astype(f32).astype(bf16), normed_ref[...])
+            out_ref[2 * i + k] = picked.astype(bf16)
+            if o == 0 and k == 0:
+                pltpu.make_async_copy(out_ref.at[2 * i + k], arrived.at[me], drecv.at[me]).start()
+            else:
+                remote(
+                    out_ref.at[2 * i + k],
+                    arrived.at[me],
+                    dsend.at[2 * i + k],
+                    drecv.at[me],
+                    {"sp": peer},
+                )
+
+    def buffers(i):
+        if i == shared:
             return s_pre, s_pre_in, s_hid
-        return pre.at[c], pre_in.at[c], hid.at[c]
-
-    def send_pre(c):
-        here, there, _ = buffers(c)
-        for d in range(1, n_tp):
-            peer = lax.rem(col + d, n_tp)
-            for k in range(2):
-                remote(
-                    here.at[k, :, slab(peer)],
-                    there.at[d - 1, k],
-                    psend.at[c, d - 1, k],
-                    precv.at[c, d - 1, k],
-                    {"tp": peer},
-                )
-
-    def first(c):
-        here, _, _ = buffers(c)
-        if c == shared:
-            rows = normed_ref[...]
-            here[0] = dot(rows, sg_ref[...]).astype(bf16)
-            here[1] = dot(rows, su_ref[...]).astype(bf16)
+        return pre.at[i], pre_in.at[i], hid.at[i]
+
+    def first(i):
+        here, there, _ = buffers(i)
+        if i == shared:
+            loads[6].wait()
+            loads[7].wait()
+            for k, weight in enumerate((sg_ref, su_ref)):
+                here[k] = dot(normed_ref[...], weight[...]).astype(bf16)
         else:
             grouped = None
             for k in range(2):
-                source = chips[c] * 2 + k
-                slot = arrived.at[source]
-                pltpu.make_async_copy(slot, slot, drecv.at[source]).wait()
+                source = chips[i] * 2 + k
+                landed(arrived.at[source], drecv.at[source])
                 term = dot(gather_ref[:, k * LANES : k * LANES + block], arrived[source])
                 grouped = term if grouped is None else grouped + term
             grouped = grouped.astype(bf16)
             tall = grouped.shape[0] // experts
-            if c == 0:
-                loads[0].wait()
-                loads[1].wait()
-            for k in range(2):
-                parts = [
-                    dot(grouped[e * tall : (e + 1) * tall], weights[k, e]).astype(bf16)
+            if i == 0:
+                loads[3].wait()
+                loads[4].wait()
+            for k, weight in enumerate((w_gate, w_up)):
+                terms = [
+                    dot(grouped[e * tall : (e + 1) * tall], weight[e]).astype(bf16)
                     for e in range(experts)
                 ]
-                spread_rows = jnp.concatenate(parts, axis=0)
+                spread_rows = jnp.concatenate(terms, axis=0)
                 here[k] = jnp.concatenate(
                     [dot(scatter_ref[j], spread_rows) for j in range(2)], axis=0
                 ).astype(bf16)
-        send_pre(c)
-
-    def second(c):
-        here, there, full = buffers(c)
+        for d in range(1, n_tp):
+            for k in range(2):
+                remote(
+                    here.at[k, :, columns(peers[d - 1], part)],
+                    there.at[d - 1, k],
+                    psend.at[i, d - 1, k],
+                    precv.at[i, d - 1, k],
+                    {"tp": peers[d - 1]},
+                )
+
+    def second(i):
+        here, there, whole = buffers(i)
         sums = []
         for k in range(2):
-            total = here[k, :, slab(col)].astype(f32)
+            total = here[k, :, columns(col, part)].astype(f32)
             for d in range(1, n_tp):
-                slot = there.at[d - 1, k]
-                pltpu.make_async_copy(slot, slot, precv.at[c, d - 1, k]).wait()
+                landed(there.at[d - 1, k], precv.at[i, d - 1, k])
                 total = total + there[d - 1, k].astype(f32)
             sums.append(total)
-        full[:, slab(col)] = (sums[0] / (1.0 + jnp.exp(-sums[0])) * sums[1]).astype(bf16)
+        whole[:, columns(col, part)] = (sums[0] / (1.0 + jnp.exp(-sums[0])) * sums[1]).astype(bf16)
         for d in range(1, n_tp):
-            peer = lax.rem(col + d, n_tp)
-            mine = full.at[:, slab(col)]
-            remote(mine, mine, hsend.at[c, d - 1], hrecv.at[c, d - 1], {"tp": peer})
-
-    def third(c):
-        _, _, full = buffers(c)
+            mine = whole.at[:, columns(col, part)]
+            remote(mine, mine, hsend.at[i, d - 1], hrecv.at[i, d - 1], {"tp": peers[d - 1]})
+
+    kept = []
+
+    def third(i):
+        _, _, whole = buffers(i)
         for d in range(1, n_tp):
-            slot = full.at[:, slab(lax.rem(col + n_tp - d, n_tp))]
-            pltpu.make_async_copy(slot, slot, hrecv.at[c, d - 1]).wait()
-        if c == shared:
-            result_sum = dot(full[...], sd_ref[...])
-            return result_sum
-        hidden = full[...]
+            source = lax.rem(col + n_tp - d, n_tp)
+            landed(whole.at[:, columns(source, part)], hrecv.at[i, d - 1])
+        if i == shared:
+            loads[8].wait()
+            result_ref[...] = result_ref[...] + dot(whole[...], sd_ref[...])
+            return
+        hidden = whole[...]
         grouped = dot(gather_ref[:, :block], hidden[:block]) + dot(
             gather_ref[:, LANES : LANES + block], hidden[block:]
         )
         grouped = grouped.astype(bf16)
         tall = grouped.shape[0] // experts
-        if c == 0:
-            loads[2].wait()
-        parts = [
-            dot(grouped[e * tall : (e + 1) * tall], weights[2, e]).astype(bf16)
-            for e in range(experts)
+        if i == 0:
+            loads[5].wait()
+        terms = [
+            dot(grouped[e * tall : (e + 1) * tall], w_down[e]).astype(bf16) for e in range(experts)
         ]
-        parts = jnp.concatenate(parts, axis=0)
+        terms = jnp.concatenate(terms, axis=0)
         for k in range(2):
-            source = chips[c] * 2 + k
-            made[c, k] = dot(scatter_ref[k], parts).astype(bf16)
-            if c == 0:
+            source = chips[i] * 2 + k
+            made_back[i, k] = dot(scatter_ref[k], terms).astype(bf16)
+            if order[i] == 0:
 
                 @pl.when(source != me)
                 def _():
                     pltpu.make_async_remote_copy(
-                        src_ref=made.at[c, k],
+                        src_ref=made_back.at[i, k],
                         dst_ref=returned.at[me],
-                        send_sem=bsend.at[c, k],
+                        send_sem=bsend.at[i, k],
                         recv_sem=brecv.at[me],
                         device_id={"sp": source},
                         device_id_type=MESH,
@@ -501,107 +729,128 @@
 
                 @pl.when(source == me)
                 def _():
-                    pltpu.make_async_copy(made.at[c, k], returned.at[me], brecv.at[me]).start()
-
+                    pltpu.make_async_copy(made_back.at[i, k], returned.at[me], brecv.at[me]).start()
+
+                kept.append((i, k, source))
             else:
                 remote(
-                    made.at[c, k], returned.at[me], bsend.at[c, k], brecv.at[me], {"sp": source}
+                    made_back.at[i, k],
+                    returned.at[me],
+                    bsend.at[i, k],
+                    brecv.at[me],
+                    {"sp": source},
                 )
-        return None
+
+    top_count = routes_ref.shape[0]
+    turned = aux[...].T[:rows]
+    taken = lax.broadcasted_iota(jnp.int32, (rows, block), 1)
+
+    def combine(i):
+        total = result_ref[...]
+        for k in range(2):
+            source = chips[i] * 2 + k
+            landed(returned.at[source], brecv.at[source])
+            seats = (taken + source * block).astype(f32)
+            gated = jnp.zeros(seats.shape, f32)
+            for t in range(top_count):
+                gate = turned[:, top_count + t : top_count + t + 1]
+                gated = gated + jnp.where(seats == turned[:, t : t + 1], gate, 0.0)
+            high = gated.astype(bf16)
+            low = (gated - high.astype(f32)).astype(bf16)
+            total = total + dot(high, returned[source]) + dot(low, returned[source])
+        result_ref[...] = total
 
     first(shared)
     first(0)
     second(shared)
-    for c in range(shared + 2):
-        if 1 <= c < shared:
-            first(c)
-        if 1 <= c <= shared:
-            second(c - 1)
-        if c == 1:
-            total = third(shared) + stream_ref[...].astype(f32)
-        if c >= 2:
-            third(c - 2)
-    for chip in chips:
-        for k in range(2):
-            source = chip * 2 + k
-            slot = returned.at[source]
-            pltpu.make_async_copy(slot, slot, brecv.at[source]).wait()
-            rows = returned[source]
-            seats = source * block + lax.broadcasted_iota(jnp.int32, (total.shape[0], block), 1)
-            gated = jnp.zeros(seats.shape, f32)
-            for t in range(slot_ref.shape[1]):
-                gated = gated + jnp.where(
-                    seats == slot_ref[:, t : t + 1], gates_ref[:, t : t + 1], 0.0
-                )
-            high = gated.astype(bf16)
-            low = (gated - high.astype(f32)).astype(bf16)
-            total = total + dot(high, rows) + dot(low, rows)
-    result_ref[...] = total.astype(bf16)
+    for i in range(1, shared + 2):
+        if i < shared:
+            first(i)
+        if i <= shared:
+            second(i - 1)
+        if i == 1:
+            third(shared)
+        else:
+            third(i - 2)
+    for i in range(shared):
+        combine(i)
     for copy in sends:
         copy.wait_send()
-    for k in range(2):
-
-        @pl.when(chips[0] * 2 + k != me)
-        def _():
-            pltpu.make_async_copy(made.at[0, k], made.at[0, k], bsend.at[0, k]).wait()
-
-
-def moe_fused(n_sp, n_tp, outgoing, normed, stream, slot, gates, capacity, mats, shared_mats, cid):
-    bf16 = jnp.bfloat16
-    experts, hidden_width = mats[0].shape[0], mats[0].shape[2]
-    block, width = outgoing.shape[1], outgoing.shape[2]
-    rows = normed.shape[0]
+    for g, m, block_q in backs:
+
+        @pl.when(block_q != me)
+        def _(g=g, m=m):
+            landed(made[g].at[m], osend.at[g, m])
+
+    for i, k, source in kept:
+
+        @pl.when(source != me)
+        def _(i=i, k=k):
+            landed(made_back.at[i, k], bsend.at[i, k])
+
+
+def layer(n_sp, n_tp, groups, capacity, arrays, small, large):
+    f32, bf16 = jnp.float32, jnp.bfloat16
+    rows = arrays[0].shape[0]
+    resid, w_gate = large[2], large[3]
+    width = resid.shape[1]
+    experts, hidden_width = w_gate.shape[0], w_gate.shape[2]
+    block = experts * capacity
     nz = n_sp // 2
+    order = (0,) + tuple(range(nz - 1, 0, -1))
+    wide = -(-rows // LANES) * LANES
+    lines = -(-(small[0].shape[0] + small[1].shape[0]) // 8) * 8
     tall = -(-2 * capacity // 16) * 16
-    index = np.arange(block)
-    gather = np.zeros((experts * tall, 2 * LANES), np.float32)
-    scatter = np.zeros((2, block, experts * tall), np.float32)
-    for k in range(2):
-        place = index // capacity * tall + k * capacity + index % capacity
-        gather[place, k * LANES + index] = 1.0
-        scatter[k, index, place] = 1.0
     part = hidden_width // n_tp
     dma = pltpu.SemaphoreType.DMA
+    vmem = pltpu.VMEM
     anywhere = pl.BlockSpec(memory_space=pl.ANY)
+    scratch = (
+        [vmem((n_sp * rows, LANES), bf16)] * 6
+        + [vmem((n_sp * lines, wide), f32)]
+        + [vmem((nz, rows, LANES), bf16)] * 2
+        + [vmem((rows, units * LANES), bf16) for units, _ in groups]
+        + [vmem(a.shape, a.dtype) for a in large]
+        + [
+            vmem((lines, wide), f32),
+            vmem((n_tp, rows, width), f32),
+            vmem((n_tp, rows, width), bf16),
+            vmem((n_tp - 1, rows, width), bf16),
+            vmem((LANES, wide), f32),
+            vmem((8, wide), f32),
+            vmem((n_tp - 1, 8, wide), f32),
+            vmem((rows, width), bf16),
+        ]
+        + [
+            vmem((n_sp, block, width), bf16),
+            vmem((n_sp, block, width), bf16),
+            vmem((n_sp, block, width), bf16),
+            vmem((nz, 2, block, width), bf16),
+            vmem((nz, 2, 2 * block, hidden_width), bf16),
+            vmem((nz, n_tp - 1, 2, 2 * block, part), bf16),
+            vmem((nz, 2 * block, hidden_width), bf16),
+            vmem((2, rows, hidden_width), bf16),
+            vmem((n_tp - 1, 2, rows, part), bf16),
+            vmem((rows, hidden_width), bf16),
+        ]
+        + [vmem((experts * tall, 2 * LANES), bf16), vmem((2, block, experts * tall), bf16)]
+        + [dma((len(large),))]
+        + [dma((nz, 7))] * 4
+        + [dma((2, nz))] * 2
+        + [dma((n_tp - 1,))] * 4
+        + [dma((n_sp,)), dma((n_sp,)), dma((nz, 2)), dma((n_sp,))]
+        + [dma((nz + 1, n_tp - 1, 2))] * 2
+        + [dma((nz + 1, n_tp - 1))] * 2
+    )
     return pl.pallas_call(
-        functools.partial(moe_kernel, n_sp, n_tp),
-        out_shape=jax.ShapeDtypeStruct((rows, width), bf16),
-        in_specs=[VM] * 7 + [anywhere] * 3 + [VM] * 3,
+        functools.partial(layer_kernel, n_sp, n_tp, groups, capacity, order),
+        out_shape=jax.ShapeDtypeStruct((rows, width), f32),
+        in_specs=[VM] * 12 + [anywhere] * 9,
         out_specs=VM,
-        scratch_shapes=[
-            pltpu.VMEM((n_sp, block, width), bf16),
-            pltpu.VMEM((n_sp, block, width), bf16),
-            pltpu.VMEM((nz, 2, block, width), bf16),
-            pltpu.VMEM((nz, 2, 2 * block, hidden_width), bf16),
-            pltpu.VMEM((nz, n_tp - 1, 2, 2 * block, part), bf16),
-            pltpu.VMEM((nz, 2 * block, hidden_width), bf16),
-            pltpu.VMEM((2, rows, hidden_width), bf16),
-            pltpu.VMEM((n_tp - 1, 2, rows, part), bf16),
-            pltpu.VMEM((rows, hidden_width), bf16),
-            pltpu.VMEM((3,) + mats[0].shape, bf16),
-            dma((3,)),
-            dma((n_sp,)),
-            dma((n_sp,)),
-            dma((nz, 2)),
-            dma((n_sp,)),
-            dma((nz + 1, n_tp - 1, 2)),
-            dma((nz + 1, n_tp - 1, 2)),
-            dma((nz + 1, n_tp - 1)),
-            dma((nz + 1, n_tp - 1)),
-        ],
-        compiler_params=params(cid),
-        name="moe",
-    )(
-        outgoing,
-        normed,
-        stream,
-        slot,
-        gates,
-        jnp.asarray(gather, bf16),
-        jnp.asarray(scatter, bf16),
-        *mats,
-        *shared_mats,
-    )
+        scratch_shapes=scratch,
+        compiler_params=params(9),
+        name="layer",
+    )(*arrays, *small, *large)
 
 
 def shards(
@@ -640,6 +889,25 @@
     experts = local_experts * n_sp
     top_count = routes.shape[1]
     capacity = max(1, (3 * rows * top_count + 2 * experts - 1) // (2 * experts))
+    block = local_experts * capacity
+    hidden_width = exp_gate.shape[2]
+    groups = ((units_a, query_a.shape[1] // heads_a), (units_b, query_b.shape[1] // heads_b))
+    fused = (
+        (hidden_width // n_tp) % LANES == 0
+        and width % LANES == 0
+        and block % 8 == 0
+        and block <= LANES
+        and exp_gate.shape == exp_down.shape
+        and all(2 * units == n_sp for units, _ in groups)
+        and (n_sp // 2) & (n_sp // 2 - 1) == 0
+        and 2 * rows <= 4 * LANES
+    )
+    if fused:
+        arrays = (query_a, key_a, value_a, query_b, key_b, value_b)
+        small = (stop_a.T, stop_b.T, routes.T, gates.T, mix_gain[None, :], ffn_gain[None, :])
+        large = (out_a, out_b, resid, exp_gate, exp_up, exp_down, sh_gate, sh_up, sh_down)
+        return layer(n_sp, n_tp, groups, capacity, arrays, small, large).astype(bf16)
+
     flat_routes = routes.reshape(-1)
     onehot = (flat_routes[:, None] == jnp.arange(experts, dtype=jnp.int32)[None, :]).astype(f32)
     pairs = rows * top_count
@@ -648,14 +916,6 @@
     slot = flat_routes * capacity + jnp.sum(earlier * onehot, axis=1).astype(jnp.int32)
     slot = slot.reshape(rows, top_count)
     slots = jnp.arange(experts * capacity, dtype=jnp.int32)
-    block = local_experts * capacity
-    hidden_width = exp_gate.shape[2]
-    fused = (
-        (hidden_width // n_tp) % LANES == 0
-        and block % 8 == 0
-        and block <= LANES
-        and exp_gate.shape == exp_down.shape
-    )
     chosen = slot[:, :, None] == slots[None, None, :]
     chooser = jnp.sum(chosen.astype(f32), axis=1).astype(bf16)
     gated = jnp.sum(jnp.where(chosen, gates[:, :, None], 0.0), axis=1)
@@ -666,7 +926,6 @@
     lines = -(-stops.shape[1] // 8) * 8
     wide = -(-rows // LANES) * LANES
     stops = jnp.pad(stops.T, ((0, lines - stops.shape[1]), (0, wide - rows)))
-    groups = ((units_a, query_a.shape[1] // heads_a), (units_b, query_b.shape[1] // heads_b))
     arrays = (query_a, key_a, value_a, query_b, key_b, value_b, stops)
     attended_a, attended_b = stick(n_sp, rows, arrays, groups, (0, heads_a), 0)
 
@@ -695,20 +954,6 @@
 
     outgoing = lax.dot_general(chooser, normed, (((0,), (0,)), ((), ())), preferred_element_type=f32)
     outgoing = outgoing.astype(bf16).reshape(n_sp, local_experts * capacity, width)
-    if fused:
-        return moe_fused(
-            n_sp,
-            n_tp,
-            outgoing,
-            normed,
-            stream,
-            slot,
-            gates,
-            capacity,
-            (exp_gate, exp_up, exp_down),
-            (sh_gate, sh_up, sh_down),
-            8,
-        )
     (arrived,) = exchange("sp", n_sp, (outgoing,), ("lead",), 4)
     arrived = arrived.reshape(n_sp, local_experts, capacity, width)
     arrived = jnp.transpose(arrived, (1, 0, 2, 3)).reshape(local_experts, n_sp * capacity, width)

time: 136 us -> 108 us (0.79)
  Pallas kernels: 123 us -> 106 us
  matrix products: 4.52 us -> 0 us
  local copies, waits for them, and re-layouts: 3.62 us -> 0 us
  other arithmetic: 4.85 us -> 1.7 us
    pallas_call x4 -> x1, Pallas kernels: 123 us -> 106 us  [layer(): pl.pallas_call(functools.partial(layer_kernel, n_sp, n_tp, groups, capaci...]
    dot_general x4 -> x0, matrix products: 4.52 us -> none  [the longest x1 1.66 us: shards(): partial_value = jnp.dot(attended_a, out_a, preferred_element_type=f32)]
    unnamed x23 -> x0, local copies, waits for them, and re-layouts: 2.53 us -> none
    reduce_sum x4 -> x0, other arithmetic: 2.48 us -> none  [the longest x1 1.28 us: shards(): mixed = jnp.sum(pieces.astype(f32), axis=0)]
where the time goes in v1:
time: 108 us
  Pallas kernels  106 us (98%)
  other arithmetic  1.7 us (2%)
    pallas_call x1, Pallas kernels, layer(): pl.pallas_call(functools.partial(layer_kernel, n_sp, n_tp, groups, capaci...  106 us

profile of v1, /device:TPU:1, one launch (start us, length us, event | category | flops | bytes accessed | tf_op | source)
XLA Modules:
  0.0 107.5 jit_solution(16311495410221948201)
XLA Ops:
  0.0 105.8 %layer.1 = f32[192,512]{1,0:T(8,128)} custom-call(bf16[192,512]{1,0:T(8,128)(2,1)} %refs_0_.1, bf16[192,512]{1,0:T(8,128)(2,1)} %refs_1_.1, bf16[192,512]{1,0:T(8,128)(2,1)} %refs_2_.1, bf16[192,512]{1,0:T(8,128)(2,1)} %refs_3_.1, bf16[192,512]{1,0:T(8,128)(2,1)} %refs_4_.1, bf16[192,512]{1,0:T(8,128)(2,1)} %refs_5_.1, f32[8,192]{1,0:T(8,128)} %bitcast.6, ...), custom_call_target="tpu_custom_call" | custom-call | tf_op jit(solution)/shard_map/layer/pallas_call | solution.py:845
  105.8 1.7 %convert_element_type.3 = bf16[192,512]{1,0:T(8,128)(2,1)} convert(f32[192,512]{1,0:T(8,128)} %layer.1) | non-fusion elementwise | flops 98304 | bytes 589824 | tf_op jit(solution)/shard_map/convert_element_type | solution.py:909

commit v2 on v1

--- a/solution.py
+++ b/solution.py
@@ -386,6 +386,7 @@
         )
         copy.start()
         sends.append(copy)
+        return copy
 
     def landed(ref, sem):
         pltpu.make_async_copy(ref, ref, sem).wait()
@@ -403,10 +404,12 @@
         return full[t].at[pl.ds(pl.multiple_of(source * tall, tall), tall), :]
 
     places = [flip(z, o) for o in range(nz)]
-    for g in range(2):
+    pushed = {}
+
+    def push(g):
         for t in names[g]:
             for o in range(1, nz):
-                remote(
+                pushed[t, o] = remote(
                     piece(t, places[o]),
                     spot(t, me),
                     fsend.at[o, t],
@@ -414,6 +417,8 @@
                     {"sp": places[o] * 2 + c},
                 )
             pltpu.make_async_copy(piece(t, z), spot(t, me), frecv.at[z, t]).start()
+
+    push(0)
     for load in loads:
         load.start()
 
@@ -478,10 +483,13 @@
     backs = []
     steps = [(g, m) for g in range(2) for m in range(nz)]
     offsets = (0, heads_a)
-    relay(0, 0)
     tables()
-    relayed(0, 0)
+    for o in range(nz):
+        if o == nz - 1:
+            push(1)
+        relay(0, places[o])
     for number, (g, m) in enumerate(steps):
+        relayed(g, m)
         size = groups[g][1]
         heads = LANES // size
         q_ref, k_ref, v_ref = full[3 * g : 3 * g + 3]
@@ -501,8 +509,9 @@
             carry = jnp.zeros((rows, 1), f32)
             total = jnp.zeros((rows, LANES), f32)
             for i in range(count):
-                if h == heads - 1 and i == count // 2 and number + 1 < len(steps):
-                    relay(*steps[number + 1])
+                if (g, m, h, i) == (0, nz - 1, heads - 1, count // 2):
+                    for o in range(nz):
+                        relay(1, places[o])
                 begin = block_q * rows + rows - tile * (i + 1)
                 short = (2 * m + 1) * rows - tile * (i + 1) < 0
                 short = short or (2 * m + 2) * rows - tile * (i + 1) < 0
@@ -514,17 +523,15 @@
                     mine, keys, (((1,), (1,)), ((), ())), preferred_element_type=f32
                 )
                 score = score * scale + stop
-                small = jnp.log2(1.0 + jnp.exp2(-jnp.abs(score)))
-                fail = jnp.maximum(score, 0.0) + small
+                fail = jnp.log2(1.0 + jnp.exp2(jnp.minimum(score, 100.0)))
+                fail = jnp.maximum(fail, score)
                 hit = score - fail
                 if masked:
                     valid = column < begin + tile - start
                     if i == 0:
                         valid = column + start < line + block_q * rows
                     fail = jnp.where(valid, fail, 0.0)
-                high = fail.astype(bf16)
-                low = (fail - high.astype(f32)).astype(bf16)
-                after = dot(high, upper) + dot(low, upper)
+                after = dot(fail.astype(bf16), upper)
                 weight = jnp.exp2(hit - after - carry)
                 if masked:
                     weight = jnp.where(valid, weight, 0.0)
@@ -553,8 +560,6 @@
         def _(g=g, m=m, place=place):
             pltpu.make_async_copy(made[g].at[m], place, orecv.at[g, z]).start()
 
-        if number + 1 < len(steps):
-            relayed(*steps[number + 1])
 
     loads[0].wait()
     loads[1].wait()
@@ -772,7 +777,9 @@
             third(shared)
         else:
             third(i - 2)
-    for i in range(shared):
+        if i >= 4:
+            combine(i - 4)
+    for i in range(max(shared - 2, 0), shared):
         combine(i)
     for copy in sends:
         copy.wait_send()
@@ -797,7 +804,7 @@
     experts, hidden_width = w_gate.shape[0], w_gate.shape[2]
     block = experts * capacity
     nz = n_sp // 2
-    order = (0,) + tuple(range(nz - 1, 0, -1))
+    order = tuple(range(nz // 2, nz)) + tuple(range(nz // 2 - 1, -1, -1))
     wide = -(-rows // LANES) * LANES
     lines = -(-(small[0].shape[0] + small[1].shape[0]) // 8) * 8
     tall = -(-2 * capacity // 16) * 16
@@ -844,7 +851,7 @@
     )
     return pl.pallas_call(
         functools.partial(layer_kernel, n_sp, n_tp, groups, capacity, order),
-        out_shape=jax.ShapeDtypeStruct((rows, width), f32),
+        out_shape=pltpu.VMEM((rows, width), f32),
         in_specs=[VM] * 12 + [anywhere] * 9,
         out_specs=VM,
         scratch_shapes=scratch,

time: 108 us -> 99.4 us (0.920)
  Pallas kernels: 106 us -> 98.5 us
    pallas_call x1, Pallas kernels: 106 us -> 98.5 us  [layer(): pl.pallas_call(functools.partial(layer_kernel, n_sp, n_tp, groups, capaci...]
where the time goes in v2:
time: 99.4 us; the launch traced here: 99.3 us
  Pallas kernels  98.5 us (99%)
    pallas_call x1, Pallas kernels, layer(): pl.pallas_call(functools.partial(layer_kernel, n_sp, n_tp, groups, capaci...  98.5 us

profile of v2, /device:TPU:1, one launch (start us, length us, event | category | flops | bytes accessed | tf_op | source)
XLA Modules:
  0.0 99.3 jit_solution(14299120270450558906)
XLA Ops:
  0.0 98.5 %layer.1 = f32[192,512]{1,0:T(8,128)S(1)} custom-call(bf16[192,512]{1,0:T(8,128)(2,1)} %refs_0_.1, bf16[192,512]{1,0:T(8,128)(2,1)} %refs_1_.1, bf16[192,512]{1,0:T(8,128)(2,1)} %refs_2_.1, bf16[192,512]{1,0:T(8,128)(2,1)} %refs_3_.1, bf16[192,512]{1,0:T(8,128)(2,1)} %refs_4_.1, bf16[192,512]{1,0:T(8,128)(2,1)} %refs_5_.1, f32[8,192]{1,0:T(8,128)} %bitcast.6, ...), custom_call_target="tpu_custom_call" | custom-call | tf_op jit(solution)/shard_map/layer/pallas_call | solution.py:852
  98.6 0.7 convert_element_type.3

commit v3 on v2

--- a/solution.py
+++ b/solution.py
@@ -324,6 +324,9 @@
     large, refs = refs[:9], refs[9:]
     result_ref, refs = refs[0], refs[1:]
     full, refs = refs[:7], refs[7:]
+    near, refs = refs[:6], refs[6:]
+    home, refs = refs[:4], refs[4:]
+    left_refs, refs = refs[:2], refs[2:]
     made, refs = refs[:2], refs[2:]
     attended, refs = refs[:2], refs[2:]
     held, refs = refs[:9], refs[9:]
@@ -340,13 +343,14 @@
         refs[:11],
         refs[11:],
     )
-    dsend, drecv, bsend, brecv, psend, precv, hsend, hrecv = refs
+    dsend, drecv, bsend, brecv, psend, precv, hsend, hrecv, nsend, nrecv = refs
 
     me, col = lax.axis_index("sp"), lax.axis_index("tp")
     nz = n_sp // 2
     z, c = me // 2, lax.rem(me, 2)
     partner = z * 2 + 1 - c
     rows = pieces[0].shape[0]
+    own = pl.ds(pl.multiple_of(c * rows, rows), rows)
     tall_rows = rows // LANES * LANES + (LANES if rows % LANES else 0)
     w_out_a, w_out_b, resid_ref, w_gate, w_up, w_down, sg_ref, su_ref, sd_ref = held
     experts = w_gate.shape[0]
@@ -357,6 +361,14 @@
     def dot(a, b):
         return jnp.dot(a, b, preferred_element_type=f32)
 
+    taken_in = [
+        pltpu.make_async_copy(
+            a, near[t] if t % 3 == 0 else near[t].at[own, :], load_sem.at[len(large) + t]
+        )
+        for t, a in enumerate(pieces)
+    ]
+    for copy in taken_in:
+        copy.start()
     loads = [pltpu.make_async_copy(a, b, load_sem.at[i]) for i, (a, b) in enumerate(zip(large, held))]
     stops_own[...] = jnp.zeros_like(stops_own)
     heads_a, heads_b = stop_a.shape[0], stop_b.shape[0]
@@ -391,45 +403,64 @@
     def landed(ref, sem):
         pltpu.make_async_copy(ref, ref, sem).wait()
 
-    ins = tuple(pieces) + (stops_own,)
-    names = ((6, 0, 1, 2), (3, 4, 5))
+    ends = nz - 1
+    names = ((6, 0), (1, 2)), ((3,), (4, 5))
 
     def piece(t, place):
         if t == 6:
-            return ins[t]
-        return ins[t].at[:, pl.ds(pl.multiple_of(place * LANES, LANES), LANES)]
+            return stops_own
+        lanes = pl.ds(pl.multiple_of(place * LANES, LANES), LANES)
+        return near[t].at[:, lanes] if t % 3 == 0 else near[t].at[own, lanes]
 
     def spot(t, source):
-        tall = ins[t].shape[0]
+        tall = stops_own.shape[0] if t == 6 else rows
         return full[t].at[pl.ds(pl.multiple_of(source * tall, tall), tall), :]
 
     places = [flip(z, o) for o in range(nz)]
-    pushed = {}
 
     def push(g):
-        for t in names[g]:
-            for o in range(1, nz):
-                pushed[t, o] = remote(
-                    piece(t, places[o]),
-                    spot(t, me),
-                    fsend.at[o, t],
-                    frecv.at[z, t],
-                    {"sp": places[o] * 2 + c},
-                )
-            pltpu.make_async_copy(piece(t, z), spot(t, me), frecv.at[z, t]).start()
-
+        for part_names, needed in ((names[g][1], z < ends), (names[g][0], z > 0)):
+
+            @pl.when(needed)
+            def _(part_names=part_names):
+                for t in part_names:
+                    for o in range(1, nz):
+                        pltpu.make_async_remote_copy(
+                            src_ref=piece(t, places[o]),
+                            dst_ref=spot(t, me),
+                            send_sem=fsend.at[o, t],
+                            recv_sem=frecv.at[z, t],
+                            device_id={"sp": places[o] * 2 + c},
+                            device_id_type=MESH,
+                        ).start()
+                    pltpu.make_async_copy(piece(t, z), spot(t, me), frecv.at[z, t]).start()
+
+    def pushed(g):
+        for part_names, needed in ((names[g][1], z < ends), (names[g][0], z > 0)):
+
+            @pl.when(needed)
+            def _(part_names=part_names):
+                for t in part_names:
+                    for o in range(1, nz):
+                        landed(piece(t, places[o]), fsend.at[o, t])
+
+    for copy in taken_in:
+        copy.wait()
+    for t in (1, 2, 4, 5):
+        mine = near[t].at[own, :]
+        remote(mine, mine, nsend.at[t], nrecv.at[t], {"sp": partner})
     push(0)
     for load in loads:
         load.start()
 
     def relay(g, chip):
-        for t in names[g]:
+        for t in names[g][1]:
             mine = spot(t, chip * 2 + c)
             landed(mine, frecv.at[chip, t])
             remote(mine, mine, rsend.at[chip, t], rrecv.at[chip, t], {"sp": partner})
 
     def relayed(g, chip):
-        for t in names[g]:
+        for t in names[g][1]:
             landed(spot(t, chip * 2 + 1 - c), rrecv.at[chip, t])
 
     slot_rows = []
@@ -472,35 +503,90 @@
             scatter_ref[k] = hit.astype(f32).astype(bf16)
 
     tile = 2 * LANES
-    upper = (
-        lax.broadcasted_iota(jnp.int32, (tile, tile), 0)
-        > lax.broadcasted_iota(jnp.int32, (tile, tile), 1)
-    ).astype(bf16)
+
+    def above(size):
+        return (
+            lax.broadcasted_iota(jnp.int32, (size, size), 0)
+            > lax.broadcasted_iota(jnp.int32, (size, size), 1)
+        ).astype(bf16)
+
     lane = lax.broadcasted_iota(jnp.int32, (rows, LANES), 1)
-    column = lax.broadcasted_iota(jnp.int32, (rows, tile), 1)
-    line = lax.broadcasted_iota(jnp.int32, (rows, tile), 0)
-
+    offsets = (0, heads_a)
+    fill = jnp.zeros((LANES - stops_own.shape[0], stops_own.shape[1]), f32)
+
+    def weigh(mine, keys, stop, scale, upper, valid, carry):
+        score = lax.dot_general(mine, keys, (((1,), (1,)), ((), ())), preferred_element_type=f32)
+        score = score * scale + stop
+        fail = jnp.log2(1.0 + jnp.exp2(jnp.minimum(score, 100.0)))
+        fail = jnp.maximum(fail, score)
+        hit = score - fail
+        if valid is not None:
+            fail = jnp.where(valid, fail, 0.0)
+        after = dot(fail.astype(bf16), upper)
+        weight = jnp.exp2(hit - after if carry is None else hit - after - carry)
+        if valid is not None:
+            weight = jnp.where(valid, weight, 0.0)
+        spent = after[:, :1] + fail[:, :1]
+        return weight.astype(bf16), spent if carry is None else carry + spent
+
+    def merge(parts, size):
+        merged = parts[0]
+        for h in range(1, len(parts)):
+            merged = jnp.where(lane // size >= h, parts[h], merged)
+        return merged
+
+    def at_home(g):
+        size = groups[g][1]
+        heads = LANES // size
+        scale = LOG2E * size ** (-0.5)
+        upper = above(2 * rows)
+        valid = lax.broadcasted_iota(jnp.int32, (rows, 2 * rows), 1) < (
+            lax.broadcasted_iota(jnp.int32, (rows, 2 * rows), 0) + c * rows
+        )
+        stop_all = jnp.concatenate([stops_own[...], fill], axis=0).T[:rows]
+        for t in (3 * g + 1, 3 * g + 2):
+            landed(near[t].at[pl.ds(pl.multiple_of((1 - c) * rows, rows), rows), :], nrecv.at[t])
+        for u in range(groups[g][0]):
+            lanes = slice(u * LANES, (u + 1) * LANES)
+            query = near[3 * g][:, lanes]
+            keys, values = near[3 * g + 1][:, lanes], near[3 * g + 2][:, lanes]
+            parts, factors = [], []
+            for h in range(heads):
+                head = offsets[g] + u * heads + h
+                stop = stop_all[:, head : head + 1] * LOG2E
+                mine = query * ((lane // size) == h).astype(bf16) if heads > 1 else query
+                weight, spent = weigh(mine, keys, stop, scale, upper, valid, None)
+                parts.append(dot(weight, values))
+                factors.append(jnp.exp2(-spent))
+            home[2 * g][:, lanes] = merge(parts, size)
+            home[2 * g + 1][:, lanes] = merge(
+                [jnp.broadcast_to(f, (rows, LANES)) for f in factors], size
+            )
+
+    tables()
+    at_home(0)
+    push(1)
+    at_home(1)
+    for chip in range(ends):
+        relay(0, chip)
+    upper = above(tile)
     backs = []
-    steps = [(g, m) for g in range(2) for m in range(nz)]
-    offsets = (0, heads_a)
-    tables()
-    for o in range(nz):
-        if o == nz - 1:
-            push(1)
-        relay(0, places[o])
-    for number, (g, m) in enumerate(steps):
-        relayed(g, m)
+    steps = [(g, m) for g in range(2) for m in range(1, nz)]
+    for g, m in steps:
+        relayed(g, m - 1)
         size = groups[g][1]
         heads = LANES // size
         q_ref, k_ref, v_ref = full[3 * g : 3 * g + 3]
         scale = LOG2E * size ** (-0.5)
-        block_q = 2 * m + (c if m % 2 == 0 else 1 - c)
-        count = -(-(2 * m + 2) * rows // tile)
+        block_q = 2 * m + c
+        for t in names[g][0]:
+            landed(spot(t, block_q), frecv.at[m, t])
         query = q_ref[pl.ds(pl.multiple_of(block_q * rows, rows), rows), :]
         lines = stops_own.shape[0]
         stop_t = full[6][pl.ds(pl.multiple_of(block_q * lines, lines), lines), :]
-        fill = jnp.zeros((LANES - lines, stop_t.shape[1]), f32)
         stop_all = jnp.concatenate([stop_t, fill], axis=0).T[:rows]
+        reach = 2 * m * rows
+        count = -(-reach // tile)
         parts = []
         for h in range(heads):
             head = offsets[g] + z * heads + h
@@ -509,43 +595,22 @@
             carry = jnp.zeros((rows, 1), f32)
             total = jnp.zeros((rows, LANES), f32)
             for i in range(count):
-                if (g, m, h, i) == (0, nz - 1, heads - 1, count // 2):
-                    for o in range(nz):
-                        relay(1, places[o])
-                begin = block_q * rows + rows - tile * (i + 1)
-                short = (2 * m + 1) * rows - tile * (i + 1) < 0
-                short = short or (2 * m + 2) * rows - tile * (i + 1) < 0
-                masked = i == 0 or short
-                start = pl.multiple_of(jnp.maximum(begin, 0), math.gcd(rows, tile))
-                keys = k_ref[pl.ds(start, tile), :]
-                values = v_ref[pl.ds(start, tile), :]
-                score = lax.dot_general(
-                    mine, keys, (((1,), (1,)), ((), ())), preferred_element_type=f32
+                if (g, m, h, i) == (0, ends, heads - 1, count // 2):
+                    for chip in range(ends):
+                        relay(1, chip)
+                stop_at = reach - tile * i
+                start = max(stop_at - tile, 0)
+                wide = stop_at - start
+                weight, carry = weigh(
+                    mine, k_ref[start:stop_at], stop, scale, upper[:wide, :wide], None, carry
                 )
-                score = score * scale + stop
-                fail = jnp.log2(1.0 + jnp.exp2(jnp.minimum(score, 100.0)))
-                fail = jnp.maximum(fail, score)
-                hit = score - fail
-                if masked:
-                    valid = column < begin + tile - start
-                    if i == 0:
-                        valid = column + start < line + block_q * rows
-                    fail = jnp.where(valid, fail, 0.0)
-                after = dot(fail.astype(bf16), upper)
-                weight = jnp.exp2(hit - after - carry)
-                if masked:
-                    weight = jnp.where(valid, weight, 0.0)
-                carry = carry + after[:, :1] + fail[:, :1]
-                total = total + dot(weight.astype(bf16), values)
+                total = total + dot(weight, v_ref[start:stop_at])
             parts.append(total)
-        merged = parts[0]
-        for h in range(1, heads):
-            merged = jnp.where(lane // size >= h, parts[h], merged)
-        made[g][m] = merged.astype(bf16)
+        made[g][m] = merge(parts, size).astype(bf16)
         place = attended[g].at[:, pl.ds(pl.multiple_of(z * LANES, LANES), LANES)]
-        backs.append((g, m, block_q))
-
-        @pl.when(block_q != me)
+        backs.append((g, m))
+
+        @pl.when(m != z)
         def _(g=g, m=m, place=place, block_q=block_q):
             pltpu.make_async_remote_copy(
                 src_ref=made[g].at[m],
@@ -556,10 +621,9 @@
                 device_id_type=MESH,
             ).start()
 
-        @pl.when(block_q == me)
+        @pl.when(m == z)
         def _(g=g, m=m, place=place):
             pltpu.make_async_copy(made[g].at[m], place, orecv.at[g, z]).start()
-
 
     loads[0].wait()
     loads[1].wait()
@@ -570,9 +634,19 @@
 
     peers = [lax.rem(col + d, n_tp) for d in range(1, n_tp)] + [col]
     for g, weights in enumerate((w_out_a, w_out_b)):
-        for u in range(groups[g][0]):
-            landed(attended[g].at[:, u * LANES : (u + 1) * LANES], orecv.at[g, u])
-        left = attended[g][...]
+        @pl.when(z == 0)
+        def _(g=g):
+            left_refs[g][...] = home[2 * g][...].astype(bf16)
+
+        @pl.when(z > 0)
+        def _(g=g):
+            for u in range(groups[g][0]):
+                lanes = slice(u * LANES, (u + 1) * LANES)
+                landed(attended[g].at[:, lanes], orecv.at[g, u])
+                far = home[2 * g + 1][:, lanes] * attended[g][:, lanes].astype(f32)
+                left_refs[g][:, lanes] = (home[2 * g][:, lanes] + far).astype(bf16)
+
+        left = left_refs[g][...]
         for i, peer in enumerate(peers):
             term = dot(left, weights[:, columns(peer, width)])
             if g == 0:
@@ -783,9 +857,11 @@
         combine(i)
     for copy in sends:
         copy.wait_send()
-    for g, m, block_q in backs:
-
-        @pl.when(block_q != me)
+    pushed(0)
+    pushed(1)
+    for g, m in backs:
+
+        @pl.when(m != z)
         def _(g=g, m=m):
             landed(made[g].at[m], osend.at[g, m])
 
@@ -815,6 +891,9 @@
     scratch = (
         [vmem((n_sp * rows, LANES), bf16)] * 6
         + [vmem((n_sp * lines, wide), f32)]
+        + [vmem(((1 if t % 3 == 0 else 2) * rows, a.shape[1]), bf16) for t, a in enumerate(arrays)]
+        + [vmem((rows, units * LANES), f32) for units, _ in groups for _ in range(2)]
+        + [vmem((rows, units * LANES), bf16) for units, _ in groups]
         + [vmem((nz, rows, LANES), bf16)] * 2
         + [vmem((rows, units * LANES), bf16) for units, _ in groups]
         + [vmem(a.shape, a.dtype) for a in large]
@@ -841,18 +920,19 @@
             vmem((rows, hidden_width), bf16),
         ]
         + [vmem((experts * tall, 2 * LANES), bf16), vmem((2, block, experts * tall), bf16)]
-        + [dma((len(large),))]
+        + [dma((len(large) + len(arrays),))]
         + [dma((nz, 7))] * 4
         + [dma((2, nz))] * 2
         + [dma((n_tp - 1,))] * 4
         + [dma((n_sp,)), dma((n_sp,)), dma((nz, 2)), dma((n_sp,))]
         + [dma((nz + 1, n_tp - 1, 2))] * 2
         + [dma((nz + 1, n_tp - 1))] * 2
+        + [dma((6,))] * 2
     )
     return pl.pallas_call(
         functools.partial(layer_kernel, n_sp, n_tp, groups, capacity, order),
         out_shape=pltpu.VMEM((rows, width), f32),
-        in_specs=[VM] * 12 + [anywhere] * 9,
+        in_specs=[anywhere] * 6 + [VM] * 6 + [anywhere] * 9,
         out_specs=VM,
         scratch_shapes=scratch,
         compiler_params=params(9),
@@ -908,6 +988,8 @@
         and all(2 * units == n_sp for units, _ in groups)
         and (n_sp // 2) & (n_sp // 2 - 1) == 0
         and 2 * rows <= 4 * LANES
+        and 2 * rows % LANES == 0
+        and rows % 16 == 0
     )
     if fused:
         arrays = (query_a, key_a, value_a, query_b, key_b, value_b)

time: 99.4 us -> 93.7 us (0.943)
  Pallas kernels: 98.5 us -> 92.8 us
    pallas_call x1, Pallas kernels: 98.5 us -> 92.8 us  [layer(): pl.pallas_call(functools.partial(layer_kernel, n_sp, n_tp, groups, capaci...]
where the time goes in v3:
time: 93.7 us; the launch traced here: 93.5 us
  Pallas kernels  92.8 us (99%)
    pallas_call x1, Pallas kernels, layer(): pl.pallas_call(functools.partial(layer_kernel, n_sp, n_tp, groups, capaci...  92.8 us

profile of v3, /device:TPU:1, one launch (start us, length us, event | category | flops | bytes accessed | tf_op | source)
XLA Modules:
  0.0 93.5 jit_solution(11901277480541210246)
XLA Ops:
  0.0 92.8 %layer.1 = f32[192,512]{1,0:T(8,128)S(1)} custom-call(bf16[192,512]{1,0:T(8,128)(2,1)} %refs_0_.1, bf16[192,512]{1,0:T(8,128)(2,1)} %refs_1_.1, bf16[192,512]{1,0:T(8,128)(2,1)} %refs_2_.1, bf16[192,512]{1,0:T(8,128)(2,1)} %refs_3_.1, bf16[192,512]{1,0:T(8,128)(2,1)} %refs_4_.1, bf16[192,512]{1,0:T(8,128)(2,1)} %refs_5_.1, f32[8,192]{1,0:T(8,128)} %bitcast.6, ...), custom_call_target="tpu_custom_call" | custom-call | tf_op jit(solution)/shard_map/layer/pallas_call | solution.py:932
  92.8 0.7 convert_element_type.3

commit v4 on v3

--- a/solution.py
+++ b/solution.py
@@ -498,9 +498,10 @@
             hit = where_of(index, k) == lax.broadcasted_iota(jnp.int32, (spread, LANES), 0)
             hit = jnp.logical_and(hit, index < block)
             gather_ref[:, k * LANES : (k + 1) * LANES] = hit.astype(f32).astype(bf16)
-            index = lax.broadcasted_iota(jnp.int32, (block, spread), 0)
-            hit = where_of(index, k) == lax.broadcasted_iota(jnp.int32, (block, spread), 1)
-            scatter_ref[k] = hit.astype(f32).astype(bf16)
+        index = lax.broadcasted_iota(jnp.int32, (2 * block, spread), 0)
+        place = jnp.where(index < block, where_of(index, 0), where_of(index - block, 1))
+        hit = place == lax.broadcasted_iota(jnp.int32, (2 * block, spread), 1)
+        scatter_ref[...] = hit.astype(f32).astype(bf16)
 
     tile = 2 * LANES
 
@@ -690,25 +691,21 @@
     chips = [flip(z, o) for o in order]
     shared = len(chips)
     seat = lax.broadcasted_iota(jnp.int32, (block, rows), 0)
-    for i, o in enumerate(order):
+
+    def dispatch(i):
         for k in range(2):
             peer = chips[i] * 2 + lax.rem(c + k, 2)
             seats = (seat + peer * block).astype(f32)
             chosen = seats == slot_rows[0]
             for slot in slot_rows[1:]:
                 chosen = jnp.logical_or(chosen, seats == slot)
-            picked = dot(chosen.astype(f32).astype(bf16), normed_ref[...])
-            out_ref[2 * i + k] = picked.astype(bf16)
-            if o == 0 and k == 0:
-                pltpu.make_async_copy(out_ref.at[2 * i + k], arrived.at[me], drecv.at[me]).start()
+            picked = dot(chosen.astype(f32).astype(bf16), normed_ref[...]).astype(bf16)
+            here = out_ref.at[2 * i + k]
+            out_ref[2 * i + k] = picked
+            if order[i] == 0 and k == 0:
+                pltpu.make_async_copy(here, arrived.at[me], drecv.at[me]).start()
             else:
-                remote(
-                    out_ref.at[2 * i + k],
-                    arrived.at[me],
-                    dsend.at[2 * i + k],
-                    drecv.at[me],
-                    {"sp": peer},
-                )
+                remote(here, arrived.at[me], dsend.at[2 * i + k], drecv.at[me], {"sp": peer})
 
     def buffers(i):
         if i == shared:
@@ -740,9 +737,7 @@
                     for e in range(experts)
                 ]
                 spread_rows = jnp.concatenate(terms, axis=0)
-                here[k] = jnp.concatenate(
-                    [dot(scatter_ref[j], spread_rows) for j in range(2)], axis=0
-                ).astype(bf16)
+                here[k] = dot(scatter_ref[...], spread_rows).astype(bf16)
         for d in range(1, n_tp):
             for k in range(2):
                 remote(
@@ -789,10 +784,10 @@
         terms = [
             dot(grouped[e * tall : (e + 1) * tall], w_down[e]).astype(bf16) for e in range(experts)
         ]
-        terms = jnp.concatenate(terms, axis=0)
+        terms = dot(scatter_ref[...], jnp.concatenate(terms, axis=0))
         for k in range(2):
             source = chips[i] * 2 + k
-            made_back[i, k] = dot(scatter_ref[k], terms).astype(bf16)
+            made_back[i, k] = terms[k * block : (k + 1) * block].astype(bf16)
             if order[i] == 0:
 
                 @pl.when(source != me)
@@ -839,22 +834,29 @@
             total = total + dot(high, returned[source]) + dot(low, returned[source])
         result_ref[...] = total
 
+    dispatch(1)
+    dispatch(0)
     first(shared)
     first(0)
+    dispatch(2)
+    dispatch(3)
+    first(1)
+    second(0)
+    first(2)
+    second(1)
+    first(3)
+    third(0)
+    second(2)
+    third(1)
+    second(3)
+    third(2)
     second(shared)
-    for i in range(1, shared + 2):
-        if i < shared:
-            first(i)
-        if i <= shared:
-            second(i - 1)
-        if i == 1:
-            third(shared)
-        else:
-            third(i - 2)
-        if i >= 4:
-            combine(i - 4)
-    for i in range(max(shared - 2, 0), shared):
-        combine(i)
+    third(3)
+    combine(0)
+    combine(1)
+    third(shared)
+    combine(2)
+    combine(3)
     for copy in sends:
         copy.wait_send()
     pushed(0)
@@ -880,7 +882,7 @@
     experts, hidden_width = w_gate.shape[0], w_gate.shape[2]
     block = experts * capacity
     nz = n_sp // 2
-    order = tuple(range(nz // 2, nz)) + tuple(range(nz // 2 - 1, -1, -1))
+    order = (0,) + tuple(range(nz // 2, nz)) + tuple(range(nz // 2 - 1, 0, -1))
     wide = -(-rows // LANES) * LANES
     lines = -(-(small[0].shape[0] + small[1].shape[0]) // 8) * 8
     tall = -(-2 * capacity // 16) * 16
@@ -919,7 +921,7 @@
             vmem((n_tp - 1, 2, rows, part), bf16),
             vmem((rows, hidden_width), bf16),
         ]
-        + [vmem((experts * tall, 2 * LANES), bf16), vmem((2, block, experts * tall), bf16)]
+        + [vmem((experts * tall, 2 * LANES), bf16), vmem((2 * block, experts * tall), bf16)]
         + [dma((len(large) + len(arrays),))]
         + [dma((nz, 7))] * 4
         + [dma((2, nz))] * 2

time: 93.7 us -> 91 us (0.971)
  Pallas kernels: 92.8 us -> 90 us
    pallas_call x1, Pallas kernels: 92.8 us -> 90 us  [layer(): pl.pallas_call(functools.partial(layer_kernel, n_sp, n_tp, groups, capaci...]
where the time goes in v4:
time: 91 us; the launch traced here: 90.8 us
  Pallas kernels  90 us (99%)
    pallas_call x1, Pallas kernels, layer(): pl.pallas_call(functools.partial(layer_kernel, n_sp, n_tp, groups, capaci...  90 us

profile of v4, /device:TPU:1, one launch (start us, length us, event | category | flops | bytes accessed | tf_op | source)
XLA Modules:
  0.0 90.8 jit_solution(17100498787882287267)
XLA Ops:
  0.0 90.0 %layer.1 = f32[192,512]{1,0:T(8,128)S(1)} custom-call(bf16[192,512]{1,0:T(8,128)(2,1)} %refs_0_.1, bf16[192,512]{1,0:T(8,128)(2,1)} %refs_1_.1, bf16[192,512]{1,0:T(8,128)(2,1)} %refs_2_.1, bf16[192,512]{1,0:T(8,128)(2,1)} %refs_3_.1, bf16[192,512]{1,0:T(8,128)(2,1)} %refs_4_.1, bf16[192,512]{1,0:T(8,128)(2,1)} %refs_5_.1, f32[8,192]{1,0:T(8,128)} %bitcast.6, ...), custom_call_target="tpu_custom_call" | custom-call | tf_op jit(solution)/shard_map/layer/pallas_call | solution.py:934
  90.1 0.7 convert_element_type.3
